TPU v7x, 256 devices: a whole 4x4x8 slice. The times are simulated.
256 devices in a mesh: ep: 64 (over z, x, core), tp: 4 (over y).
Axes of the slice: x: 4, y: 4, z: 8, core: 2. Of those that a mesh axis runs over, the one named last changes fastest.
Arguments:
- pool_in: bfloat16 [65536, 1024], P(('ep', 'tp')), may hold values from -6 to 6
- w_pool: bfloat16 [8, 128, 128], replicated, may hold values from -0.5 to 0.5
- pool_scale: float32 [1024], replicated, may hold values from 0.1 to 1.9
- w_out: bfloat16 [1024, 2048], replicated, may hold values from -0.1875 to 0.1875
- expert_in: bfloat16 [32768, 2048], P('ep'), may hold values from -6 to 6
- ffn_gain: float32 [2048], replicated, may hold values from 0.1 to 1.9
- routes: int32 [32768, 2], P('ep'), may hold values from 0 to 63, all different within a row; in each aligned block of 128 rows (0 to 127, 128 to 255, ...) at most 6 rows name the same one
- route_weight: float32 [32768, 2], P('ep'), may hold values from 0.25 to 1
- w_gate: bfloat16 [64, 2048, 1024], P('ep', None, 'tp'), may hold values from -0.125 to 0.125
- w_up: bfloat16 [64, 2048, 1024], P('ep', None, 'tp'), may hold values from -0.125 to 0.125
- w_down: bfloat16 [64, 1024, 2048], P('ep', 'tp'), may hold values from -0.1875 to 0.1875
Outputs:
- mixer_out: bfloat16 [65536, 2048], P(('ep', 'tp'))
- expert_out: bfloat16 [32768, 2048], P(('ep', 'tp'))
Inputs may be any that keep to these rules, and one draw needn't show every extreme that they name: `routes`: each row names 2 different experts. In each aligned block of 128 rows no expert is named by more than 6 rows, and in some block some expert is named by exactly 6 rows.
All inputs are finite; a program needn't handle non-finite values.
Results may differ from a plain program's by a relative error of at most 0.012.
Values may be sent and summed in bfloat16 or wider, within the bound.
No kernel may reach another device: no remote copies, remote signals or barrier semaphores. Data moves between devices by JAX's collectives and lax.ppermute only.
A program may use at most 128 MiB of HBM per device.

v0:
```python
from functools import partial

import jax
import jax.numpy as jnp
from jax import lax
from jax.experimental import pallas as pl
from jax.experimental.pallas import tpu as pltpu
from jax.sharding import PartitionSpec as P


GDIM = 128
WMAX = 16
K = 2
EPS = 0.05

CHUNKS = 2
SLOTS = 3
SUB = 8
LANES = 768
PIECE = 256
FOLD = LANES // PIECE
MAIN = 2 * LANES
WIDTH = MAIN + 2 * PIECE
EXPERTS_G = 32
GROUP = EXPERTS_G * SUB
DENSE = EXPERTS_G * SLOTS
SMALL = 16 * 1024 * 1024
LARGE = 52 * 1024 * 1024
LARGER = 53 * 1024 * 1024
BF16 = jnp.bfloat16
F32 = jnp.float32
VMEM = pl.BlockSpec(memory_space=pltpu.VMEM)
ANY = pl.BlockSpec(memory_space=pl.ANY)


def passed_along(array, axis, by):
    length = lax.axis_size(axis)
    pairs = [(i, i + by) for i in range(length) if 0 <= i + by < length]
    return lax.ppermute(array, axis, pairs)


def swapped(array, flip):
    eps, tps = lax.axis_size("ep"), lax.axis_size("tp")
    pairs = []
    for e in range(eps):
        for y in range(tps):
            other = y ^ 1 if (e + flip) % 2 == 0 else tps - 1 - y
            pairs.append((e * tps + y, e * tps + other))
    return lax.ppermute(array, ("ep", "tp"), pairs)


def window_sizes(width):
    group_of = jnp.arange(width) // GDIM
    level = group_of % 4
    return jnp.where(
        level == 0, 2.0, jnp.where(level == 1, 4.0, jnp.where(level == 2, 8.0, 16.0))
    ).astype(F32)


def pooled_rows(extended, positions):
    extent = extended.shape[0] - (WMAX - 1)
    window = window_sizes(extended.shape[1])
    running = jnp.zeros((extent, extended.shape[1]), F32)
    picked = running
    for offset in range(WMAX):
        running = running + extended[WMAX - 1 - offset : WMAX - 1 - offset + extent]
        if offset + 1 in (2, 4, 8, 16):
            picked = jnp.where(window[None, :] == offset + 1, running, picked)
    counted = jnp.minimum(positions[:, None] + 1.0, window[None, :])
    return (picked / counted - extended[WMAX - 1 :]).astype(BF16)


def as_bf16(mask):
    return mask.astype(F32).astype(BF16)


def dot(a, b):
    return jnp.dot(a, b, preferred_element_type=F32)


def slot_ranks(routes_ref, rows, tokens, base):
    first, second = routes_ref[0:1, :], routes_ref[1:2, :]
    row = lax.broadcasted_iota(jnp.int32, (rows, tokens), 0)
    expert, sub = row // SUB, row % SUB
    by_first, by_second = expert == first, expert == second
    named = by_first | by_second
    before = lax.broadcasted_iota(jnp.int32, (tokens, tokens), 0) < lax.broadcasted_iota(
        jnp.int32, (tokens, tokens), 1
    )
    rank = dot(as_bf16(named), as_bf16(before)).astype(jnp.int32) - base
    return by_first, named, rank, sub


def main_place(sub, slot, half):
    return (sub == 2 * slot + half) & (sub < 2 * SLOTS) & (slot >= 0)


def tail_place(sub, slot, piece, c):
    return (sub >= 2 * SLOTS) & ((sub - 2 * SLOTS) * FOLD + c == 2 * slot + piece) & (slot >= 0)


def tail_used(piece, c):
    return any((r * FOLD + c - piece) % 2 == 0 for r in range(SUB - 2 * SLOTS))


def send_kernel(base, own_ref, rows_hbm, gain_ref, routes_ref, out_ref, rows_ref, normed_ref, sems):
    tokens = rows_ref.shape[0]
    half = tokens // 2
    copies = []
    for n in range(2):
        here = pl.ds(pl.multiple_of(own_ref[0] * tokens + n * half, half), half)
        copies.append(
            pltpu.make_async_copy(
                rows_hbm.at[here], rows_ref.at[pl.ds(n * half, half)], sems.at[n]
            )
        )
        copies[n].start()
    _, named, rank, sub = slot_ranks(routes_ref, out_ref.shape[0], tokens, base)
    mains = jnp.concatenate([as_bf16(named & main_place(sub, rank, h)) for h in range(2)], axis=1)
    for n in range(2):
        here = slice(n * half, (n + 1) * half)
        copies[n].wait()
        features = rows_ref[here, :].astype(F32)
        inverse = lax.rsqrt(jnp.mean(features * features, axis=-1, keepdims=True) + EPS)
        normed_ref[here, :] = (features * inverse * gain_ref[...]).astype(BF16)
    for c in range(FOLD):
        used = [u for u in range(2) if tail_used(u, c)]
        tails = [as_bf16(named & tail_place(sub, rank, u, c)) for u in used]
        starts = [h * LANES + c * PIECE for h in range(2)] + [MAIN + u * PIECE for u in used]
        out_ref[:, c * PIECE : (c + 1) * PIECE] = dot(
            jnp.concatenate([mains, *tails], axis=1),
            jnp.concatenate([normed_ref[:, start : start + PIECE] for start in starts], axis=0),
        ).astype(BF16)


def send_rows(expert_in, gain, routes_t, own, experts, chunk):
    tokens = expert_in.shape[0] // lax.axis_size("tp")
    width = expert_in.shape[1]
    return pl.pallas_call(
        partial(send_kernel, chunk * SLOTS),
        out_shape=jax.ShapeDtypeStruct((experts * SUB, LANES), BF16),
        grid_spec=pltpu.PrefetchScalarGridSpec(
            num_scalar_prefetch=1,
            grid=(1,),
            in_specs=[
                ANY,
                pl.BlockSpec((1, width), lambda i, own: (0, 0)),
                pl.BlockSpec((K, tokens), lambda i, own: (0, own[0])),
            ],
            out_specs=VMEM,
            scratch_shapes=[pltpu.VMEM((tokens, width), BF16)] * 2 + [pltpu.SemaphoreType.DMA((2,))],
        ),
        cost_estimate=pl.CostEstimate(flops=2_000_000_000, bytes_accessed=2_100_000, transcendentals=128),
        name="send_rows",
    )(own, expert_in, gain.reshape(1, width), routes_t)


def places(shape, dense_axis, where):
    dense = lax.broadcasted_iota(jnp.int32, shape, dense_axis)
    row = lax.broadcasted_iota(jnp.int32, shape, 1 - dense_axis)
    return as_bf16((dense % EXPERTS_G == row // SUB) & where(row % SUB, dense // EXPERTS_G))


def main_maps(shape, dense_axis):
    return [places(shape, dense_axis, lambda sub, slot, h=h: main_place(sub, slot, h)) for h in range(2)]


def tail_maps(shape, dense_axis, c):
    return [
        places(shape, dense_axis, lambda sub, slot, u=u: tail_place(sub, slot, u, c))
        for u in range(2)
        if tail_used(u, c)
    ]


def dense_columns(c):
    starts = [h * LANES + c * PIECE for h in range(2)]
    return starts + [MAIN + u * PIECE for u in range(2) if tail_used(u, c)]


def unpack(x_ref, out_ref):
    experts = x_ref.shape[0] // SUB
    mains = main_maps((DENSE, GROUP), 0)
    tails = {}

    def put(block, g, start):
        for k in range(SLOTS):
            to = k * experts + g * EXPERTS_G
            out_ref[to : to + EXPERTS_G, start : start + PIECE] = block[
                k * EXPERTS_G : (k + 1) * EXPERTS_G
            ].astype(BF16)

    for c in range(FOLD):
        maps = jnp.concatenate(mains + tail_maps((DENSE, GROUP), 0, c), axis=0)
        for g in range(experts // EXPERTS_G):
            found = dot(maps, x_ref[g * GROUP : (g + 1) * GROUP, c * PIECE : (c + 1) * PIECE])
            for n, start in enumerate(dense_columns(c)):
                block = found[n * DENSE : (n + 1) * DENSE]
                if start < MAIN:
                    put(block, g, start)
                else:
                    tails[start, g] = tails[start, g] + block if (start, g) in tails else block
    for (start, g), block in tails.items():
        put(block, g, start)


def pack_kernel(a_ref, *refs):
    *b_refs, out_ref = refs
    experts = out_ref.shape[0] // SUB
    mains = main_maps((GROUP, DENSE), 1)
    for c in range(FOLD):
        maps = jnp.concatenate(mains + tail_maps((GROUP, DENSE), 1, c), axis=1)
        for g, b_ref in enumerate(b_refs):
            pieces = []
            for start in dense_columns(c):
                columns = slice(start, start + PIECE)
                for k in range(SLOTS):
                    at = k * experts + g * EXPERTS_G
                    own = a_ref[at : at + EXPERTS_G, columns].astype(F32)
                    other = b_ref[k * EXPERTS_G : (k + 1) * EXPERTS_G, columns].astype(F32)
                    pieces.append((own + other).astype(BF16))
            out_ref[g * GROUP : (g + 1) * GROUP, c * PIECE : (c + 1) * PIECE] = dot(
                maps, jnp.concatenate(pieces, axis=0)
            ).astype(BF16)


def pack_sum(a, parts):
    rows = a.shape[0] // SLOTS * SUB
    return pl.pallas_call(
        pack_kernel,
        out_shape=jax.ShapeDtypeStruct((rows, LANES), BF16),
        in_specs=[VMEM] * (1 + len(parts)),
        out_specs=VMEM,
        cost_estimate=pl.CostEstimate(flops=800_000_000, bytes_accessed=a.size * 6, transcendentals=0),
        compiler_params=pltpu.CompilerParams(vmem_limit_bytes=SMALL),
        name="pack_sum",
    )(a, *parts)


def ffn_kernel(*refs):
    sources, out_ref, dense_ref, held, sems = refs[:7], refs[7], refs[8], refs[9:16], refs[16]
    rows, *copies = [
        pltpu.make_async_copy(source, ref, sems.at[n])
        for n, (source, ref) in enumerate(zip(sources, held))
    ]
    rows.start()
    for copy in copies:
        copy.start()
    x_ref, ga_ref, ua_ref, gb_ref, ub_ref, da_ref, db_ref = held
    rows.wait()
    unpack(x_ref, dense_ref)
    x = dense_ref[...]
    copies[0].wait()
    copies[1].wait()
    hidden_a = (jax.nn.silu(dot(x, ga_ref[...])) * dot(x, ua_ref[...])).astype(BF16)
    copies[2].wait()
    copies[3].wait()
    hidden_b = (jax.nn.silu(dot(x, gb_ref[...])) * dot(x, ub_ref[...])).astype(BF16)
    copies[4].wait()
    copies[5].wait()
    step = 2 * PIECE
    for c in range(WIDTH // step):
        columns = slice(c * step, (c + 1) * step)
        out_ref[:, columns] = (
            dot(hidden_a, da_ref[:, columns]) + dot(hidden_b, db_ref[:, columns])
        ).astype(BF16)


def half_ffn(x, ga, gb, ua, ub, da, db):
    operands = (x, ga, ua, gb, ub, da, db)
    dense = x.shape[0] // SUB * SLOTS
    hidden = ga.shape[1] + gb.shape[1]
    return pl.pallas_call(
        ffn_kernel,
        out_shape=jax.ShapeDtypeStruct((dense, WIDTH), BF16),
        in_specs=[ANY] * 7,
        out_specs=VMEM,
        scratch_shapes=[pltpu.VMEM((dense, WIDTH), BF16)]
        + [pltpu.VMEM(operand.shape, BF16) for operand in operands]
        + [pltpu.SemaphoreType.DMA((7,))],
        cost_estimate=pl.CostEstimate(
            flops=3_500_000_000,
            bytes_accessed=x.size * 4 + 6 * ga.size * 2,
            transcendentals=dense * hidden,
        ),
        compiler_params=pltpu.CompilerParams(vmem_limit_bytes=LARGER),
        name="half_ffn",
    )(*operands)


def combine_kernel(base, own_ref, values_ref, routes_ref, weight_ref, *refs):
    del own_ref
    copy = None
    if base:
        source, out_ref, before_ref, sem = refs
        copy = pltpu.make_async_copy(source, before_ref, sem)
        copy.start()
    else:
        (out_ref,) = refs
    rows, tokens = values_ref.shape[0], out_ref.shape[0]
    routes = jnp.transpose(routes_ref[...].astype(F32)).astype(jnp.int32)
    weights = jnp.transpose(weight_ref[...])
    row = lax.broadcasted_iota(jnp.int32, (tokens, rows), 1)
    expert, sub = row // SUB, row % SUB
    by_first, by_second = expert == routes[:, 0:1], expert == routes[:, 1:2]
    named = by_first | by_second
    earlier = lax.broadcasted_iota(jnp.int32, (tokens, tokens), 1) < lax.broadcasted_iota(
        jnp.int32, (tokens, tokens), 0
    )
    slot = dot(as_bf16(earlier), as_bf16(named)).astype(jnp.int32) - base
    weight = jnp.where(
        named & (slot < SLOTS), jnp.where(by_first, weights[:, 0:1], weights[:, 1:2]), 0.0
    )
    high = weight.astype(BF16).astype(F32)
    low = weight - high

    def split(chosen):
        return [jnp.where(chosen, part, 0.0).astype(BF16) for part in (high, low)]

    totals = {}
    mains = [part for h in range(2) for part in split(main_place(sub, slot, h))]
    for c in range(FOLD):
        maps = list(mains)
        for u in range(2):
            if tail_used(u, c):
                maps += split(tail_place(sub, slot, u, c))
        found = dot(jnp.concatenate(maps, axis=0), values_ref[:, c * PIECE : (c + 1) * PIECE])
        for n, start in enumerate(dense_columns(c)):
            block = found[2 * n * tokens : (2 * n + 1) * tokens] + found[(2 * n + 1) * tokens : (2 * n + 2) * tokens]
            totals[start] = totals[start] + block if start in totals else block
    if copy is not None:
        copy.wait()
    for start, total in totals.items():
        columns = slice(start, start + PIECE)
        if copy is not None:
            total += before_ref[:, columns]
        out_ref[:, columns] = total.astype(out_ref.dtype)


def combine(chunk, values, routes_t, weight_t, own, tokens, before=None):
    rest = () if before is None else (before,)
    return pl.pallas_call(
        partial(combine_kernel, chunk * SLOTS),
        out_shape=jax.ShapeDtypeStruct((tokens, WIDTH), F32 if before is None else BF16),
        grid_spec=pltpu.PrefetchScalarGridSpec(
            num_scalar_prefetch=1,
            grid=(1,),
            in_specs=[
                VMEM,
                pl.BlockSpec((K, tokens), lambda i, own: (0, own[0])),
                pl.BlockSpec((K, tokens), lambda i, own: (0, own[0])),
            ]
            + [ANY] * len(rest),
            out_specs=VMEM if before is None else pl.BlockSpec((tokens, WIDTH), lambda i, own: (0, 0)),
            scratch_shapes=[pltpu.VMEM((tokens, WIDTH), F32), pltpu.SemaphoreType.DMA] if rest else [],
        ),
        cost_estimate=pl.CostEstimate(flops=1_500_000_000, bytes_accessed=2_100_000, transcendentals=0),
        compiler_params=pltpu.CompilerParams(vmem_limit_bytes=LARGE),
        name="combine",
    )(own, values, routes_t, weight_t, *rest)


def exchanged(rows):
    experts = rows.shape[0] // SUB
    out = lax.all_to_all(
        rows.reshape(experts, SUB, LANES), "ep", split_axis=0, concat_axis=0, tiled=True
    )
    return out.reshape(rows.shape)


def on_device(
    pool_in,
    w_pool,
    pool_scale,
    w_out,
    expert_in,
    ffn_gain,
    routes,
    route_weight,
    w_gate,
    w_up,
    w_down,
):
    rows_here = pool_in.shape[0]
    tokens = routes.shape[0] // lax.axis_size("tp")
    experts = lax.axis_size("ep") * w_gate.shape[0]
    own = lax.axis_index("tp").astype(jnp.int32).reshape(1)
    routes_t, weight_t = routes.T, route_weight.T
    before = passed_along(pool_in[rows_here - (WMAX - 1) :], ("ep", "tp"), 1)

    gate, up, down = w_gate[0], w_up[0], w_down[0]
    gate_b, up_b = swapped(gate, 0), swapped(up, 0)
    down_b = swapped(down, 0)
    ffn = lambda x: half_ffn(x, gate, gate_b, up, up_b, down, down_b)

    mine = []
    for n in range(CHUNKS):
        sent = send_rows(expert_in, ffn_gain, routes_t, own, experts, n)
        mine.append(exchanged(sent))
    expert_out = None
    for n in range(CHUNKS):
        back = []
        halves = mine[n].shape[0] // GROUP
        theirs = []
        for g in range(halves):
            theirs.append(swapped(mine[n][g * GROUP : (g + 1) * GROUP], 1))
        for g in range(halves):
            partial_sum = ffn(theirs[g])
            back.append(swapped(partial_sum, 1))
        kept = ffn(mine[n])
        results = pack_sum(kept, back)
        returned = exchanged(results)
        expert_out = combine(n, returned, routes_t, weight_t, own, tokens, expert_out)

    extended = jnp.concatenate([before, pool_in], axis=0).astype(F32)
    positions = (
        lax.axis_index(("ep", "tp")) * rows_here + jnp.arange(rows_here)
    ).astype(F32)
    pooled = pooled_rows(extended, positions)
    group_count = w_pool.shape[0]
    grouped = jnp.einsum(
        "tgc,gcd->tgd",
        pooled.reshape(rows_here, group_count, GDIM),
        w_pool,
        preferred_element_type=F32,
    )
    scaled = (grouped.reshape(rows_here, -1) * pool_scale).astype(BF16)
    mixer_out = dot(scaled, w_out).astype(BF16)
    return (mixer_out, expert_out)


def solution(mesh):
    placed = (
        P(("ep", "tp"), None),
        P(),
        P(),
        P(),
        P("ep", None),
        P(),
        P("ep", None),
        P("ep", None),
        P("ep", None, "tp"),
        P("ep", None, "tp"),
        P("ep", "tp", None),
    )
    return jax.shard_map(
        on_device,
        mesh=mesh,
        in_specs=placed,
        out_specs=(P(("ep", "tp"), None), P(("ep", "tp"), None)),
        check_vma=False,
    )
```

profile of v0, /device:TPU:1, one launch (start us, length us, event | category | flops | bytes accessed | tf_op | source)
XLA Modules:
  0.0 152.1 jit_solution(9483900070985098281)
XLA Ops:
  0.6 3.6 %send_rows.3 = bf16[512,768]{1,0:T(8,128)(2,1)} custom-call(s32[1]{0:T(128)} %bitcast.2.own_ref, bf16[512,2048]{1,0:T(8,128)(2,1)} %rows_hbm.3, f32[1,2048]{1,0:T(1,128)} %bitcast.51, s32[2,512]{1,0:T(2,128)} %bitcast.41), custom_call_target="tpu_custom_call" | custom-call | flops 2000000000 | bytes 2100000 | tf_op jit(solution)/shard_map/send_rows/pallas_call | solution.py:139
  4.2 13.0 %all-to-all-start.2 = ((bf16[64,8,768]{2,1,0:T(8,128)(2,1)}), bf16[64,8,768]{2,1,0:T(8,128)(2,1)S(1)}, u32[]{:S(2)}, u32[]{:S(2)}) async-start(bf16[64,8,768]{2,1,0:T(8,128)(2,1)} %bitcast.50), calls=%async_computation.2 | async-start | bytes 1572864 | tf_op jit(solution)/shard_map/all_to_all | solution.py:365
  17.2 2.8 %collective-permute-start.1 = (bf16[2048,256]{1,0:T(8,128)(2,1)}, bf16[2048,256]{1,0:T(8,128)(2,1)}, u32[]{:S(2)}, u32[]{:S(2)}) collective-permute-start(bf16[2048,256]{1,0:T(8,128)(2,1)} %bitcast.7.refs_1_), channel_id=1, source_target_pairs={{0,1},{1,0},{2,3},{3,2},{4,7},{5,6},{6,5},{7,4},{8,9},{9,8},{10,11... | collective-permute-start | bytes 3145736 | tf_op jit(solution)/shard_map/ppermute | solution.py:49
  20.1 2.6 %collective-permute-start.3 = (bf16[256,2048]{1,0:T(8,128)(2,1)}, bf16[256,2048]{1,0:T(8,128)(2,1)}, u32[]{:S(2)}, u32[]{:S(2)}) collective-permute-start(bf16[256,2048]{1,0:T(8,128)(2,1)} %bitcast.9.refs_5_), channel_id=1, source_target_pairs={{0,1},{1,0},{2,3},{3,2},{4,7},{5,6},{6,5},{7,4},{8,9},{9,8},{10,11... | collective-permute-start | bytes 3145736 | tf_op jit(solution)/shard_map/ppermute | solution.py:49
  22.7 3.5 %send_rows.2 = bf16[512,768]{1,0:T(8,128)(2,1)} custom-call(s32[1]{0:T(128)} %bitcast.2.own_ref, bf16[512,2048]{1,0:T(8,128)(2,1)} %rows_hbm.3, f32[1,2048]{1,0:T(1,128)} %bitcast.52, s32[2,512]{1,0:T(2,128)} %bitcast.42), custom_call_target="tpu_custom_call" | custom-call | flops 2000000000 | bytes 2100000 | tf_op jit(solution)/shard_map/send_rows/pallas_call | solution.py:139
  26.2 14.0 %all-to-all-done.2 = bf16[64,8,768]{2,1,0:T(8,128)(2,1)S(1)} async-done(((bf16[64,8,768]{2,1,0:T(8,128)(2,1)}), bf16[64,8,768]{2,1,0:T(8,128)(2,1)S(1)}, u32[]{:S(2)}, u32[]{:S(2)}) %all-to-all-start.2) | async-done | bytes 786464 | tf_op jit(solution)/shard_map/all_to_all | solution.py:365
  40.2 5.9 %all-to-all-start = ((bf16[64,8,768]{2,1,0:T(8,128)(2,1)}), bf16[64,8,768]{2,1,0:T(8,128)(2,1)S(1)}, u32[]{:S(2)}, u32[]{:S(2)}) async-start(bf16[64,8,768]{2,1,0:T(8,128)(2,1)} %bitcast.49), calls=%async_computation | async-start | bytes 1572864 | tf_op jit(solution)/shard_map/all_to_all | solution.py:365
  48.4 3.2 %collective-permute-start = (bf16[15,1024]{1,0:T(8,128)(2,1)}, bf16[15,1024]{1,0:T(8,128)(2,1)}, u32[]{:S(2)}, u32[]{:S(2)}) collective-permute-start(bf16[15,1024]{1,0:T(8,128)(2,1)} %slice.76), channel_id=1, source_target_pairs={{0,1},{1,2},{2,3},{3,4},{4,5},{5,6},{6,7},{7,8},{8,9},{9,10},{10,1... | collective-permute-start | bytes 92168 | tf_op jit(solution)/shard_map/ppermute | solution.py:39
  51.6 7.7 %collective-permute-done.3.refs_6_ = bf16[256,2048]{1,0:T(8,128)(2,1)} collective-permute-done((bf16[256,2048]{1,0:T(8,128)(2,1)}, bf16[256,2048]{1,0:T(8,128)(2,1)}, u32[]{:S(2)}, u32[]{:S(2)}) %collective-permute-start.3) | collective-permute-done | bytes 1048608 | tf_op jit(solution)/shard_map/ppermute | solution.py:49
  59.3 3.6 %half_ffn.11 = bf16[96,2048]{1,0:T(8,128)(2,1)S(1)} custom-call(bf16[256,768]{1,0:T(8,128)(2,1)S(1)} %collective-permute-done.10.refs_0_, bf16[2048,256]{1,0:T(8,128)(2,1)} %bitcast.7.refs_1_, bf16[2048,256]{1,0:T(8,128)(2,1)} %bitcast.8.refs_2_, bf16[2048,256]{1,0:T(8,128)(2,1)} %collective-permute-done.1.refs_3_, ...), custom_call_target="tpu_custom_call" | custom-call | flops 3500000000 | bytes 7077888 | tf_op jit(solution)/shard_map/half_ffn/pallas_call | solution.py:273
  63.3 3.6 %half_ffn.10 = bf16[96,2048]{1,0:T(8,128)(2,1)S(1)} custom-call(bf16[256,768]{1,0:T(8,128)(2,1)S(1)} %collective-permute-done.8.refs_0_, bf16[2048,256]{1,0:T(8,128)(2,1)} %bitcast.7.refs_1_, bf16[2048,256]{1,0:T(8,128)(2,1)} %bitcast.8.refs_2_, bf16[2048,256]{1,0:T(8,128)(2,1)} %collective-permute-done.1.refs_3_, ...), custom_call_target="tpu_custom_call" | custom-call | flops 3500000000 | bytes 7077888 | tf_op jit(solution)/shard_map/half_ffn/pallas_call | solution.py:273
  71.4 3.7 %half_ffn.9.a_ref = bf16[192,2048]{1,0:T(8,128)(2,1)S(1)} custom-call(bf16[512,768]{1,0:T(8,128)(2,1)} %bitcast.48, bf16[2048,256]{1,0:T(8,128)(2,1)} %bitcast.7.refs_1_, bf16[2048,256]{1,0:T(8,128)(2,1)} %bitcast.8.refs_2_, bf16[2048,256]{1,0:T(8,128)(2,1)} %collective-permute-done.1.refs_3_, bf16[2048,256]{1,0:T(8,128)(2,1)} %collective-permute-done.2.refs_4_, ...), custom_call_target="tpu_custom_call" | custom-call | flops 3500000000 | bytes 7864320 | tf_op jit(solution)/shard_map/half_ffn/pallas_call | solution.py:273
  75.1 1.8 %pack_sum.3 = bf16[512,768]{1,0:T(8,128)(2,1)} custom-call(bf16[192,2048]{1,0:T(8,128)(2,1)S(1)} %half_ffn.9.a_ref, bf16[96,2048]{1,0:T(8,128)(2,1)S(1)} %collective-permute-done.9.refs_0_, bf16[96,2048]{1,0:T(8,128)(2,1)S(1)} %collective-permute-done.11.refs_1_), custom_call_target="tpu_custom_call" | custom-call | flops 800000000 | bytes 2359296 | tf_op jit(solution)/shard_map/pack_sum/pallas_call | solution.py:229
  77.0 15.3 %all-to-all-start.3 = ((bf16[64,8,768]{2,1,0:T(8,128)(2,1)}), bf16[64,8,768]{2,1,0:T(8,128)(2,1)S(1)}, u32[]{:S(2)}, u32[]{:S(2)}) async-start(bf16[64,8,768]{2,1,0:T(8,128)(2,1)} %bitcast.19), calls=%async_computation.3 | async-start | bytes 1572864 | tf_op jit(solution)/shard_map/all_to_all | solution.py:365
  92.4 3.6 %half_ffn.7 = bf16[96,2048]{1,0:T(8,128)(2,1)S(1)} custom-call(bf16[256,768]{1,0:T(8,128)(2,1)S(1)} %collective-permute-done.4.refs_0_, bf16[2048,256]{1,0:T(8,128)(2,1)} %bitcast.7.refs_1_, bf16[2048,256]{1,0:T(8,128)(2,1)} %bitcast.8.refs_2_, bf16[2048,256]{1,0:T(8,128)(2,1)} %collective-permute-done.1.refs_3_, ...), custom_call_target="tpu_custom_call" | custom-call | flops 3500000000 | bytes 7077888 | tf_op jit(solution)/shard_map/half_ffn/pallas_call | solution.py:273
  99.3 3.6 %half_ffn.8 = bf16[96,2048]{1,0:T(8,128)(2,1)S(1)} custom-call(bf16[256,768]{1,0:T(8,128)(2,1)S(1)} %collective-permute-done.6.refs_0_, bf16[2048,256]{1,0:T(8,128)(2,1)} %bitcast.7.refs_1_, bf16[2048,256]{1,0:T(8,128)(2,1)} %bitcast.8.refs_2_, bf16[2048,256]{1,0:T(8,128)(2,1)} %collective-permute-done.1.refs_3_, ...), custom_call_target="tpu_custom_call" | custom-call | flops 3500000000 | bytes 7077888 | tf_op jit(solution)/shard_map/half_ffn/pallas_call | solution.py:273
  104.0 3.7 %half_ffn.6.a_ref = bf16[192,2048]{1,0:T(8,128)(2,1)S(1)} custom-call(bf16[512,768]{1,0:T(8,128)(2,1)} %bitcast.47, bf16[2048,256]{1,0:T(8,128)(2,1)} %bitcast.7.refs_1_, bf16[2048,256]{1,0:T(8,128)(2,1)} %bitcast.8.refs_2_, bf16[2048,256]{1,0:T(8,128)(2,1)} %collective-permute-done.1.refs_3_, bf16[2048,256]{1,0:T(8,128)(2,1)} %collective-permute-done.2.refs_4_, ...), custom_call_target="tpu_custom_call" | custom-call | flops 3500000000 | bytes 7864320 | tf_op jit(solution)/shard_map/half_ffn/pallas_call | solution.py:273
  107.7 2.3 %collective-permute-done.7.refs_1_ = bf16[96,2048]{1,0:T(8,128)(2,1)S(1)} collective-permute-done((bf16[96,2048]{1,0:T(8,128)(2,1)S(1)}, bf16[96,2048]{1,0:T(8,128)(2,1)S(1)}, u32[]{:S(2)}, u32[]{:S(2)}) %collective-permute-start.7) | collective-permute-done | bytes 393248 | tf_op jit(solution)/shard_map/ppermute | solution.py:49
  111.7 3.5 %all-to-all-done.3 = bf16[64,8,768]{2,1,0:T(8,128)(2,1)S(1)} async-done(((bf16[64,8,768]{2,1,0:T(8,128)(2,1)}), bf16[64,8,768]{2,1,0:T(8,128)(2,1)S(1)}, u32[]{:S(2)}, u32[]{:S(2)}) %all-to-all-start.3) | async-done | bytes 786464 | tf_op jit(solution)/shard_map/all_to_all | solution.py:365
  115.3 10.9 %all-to-all-start.1 = ((bf16[64,8,768]{2,1,0:T(8,128)(2,1)}), bf16[64,8,768]{2,1,0:T(8,128)(2,1)S(1)}, u32[]{:S(2)}, u32[]{:S(2)}) async-start(bf16[64,8,768]{2,1,0:T(8,128)(2,1)} %bitcast.12), calls=%async_computation.1 | async-start | bytes 1572864 | tf_op jit(solution)/shard_map/all_to_all | solution.py:365
  126.2 1.9 %fusion.5 = f32[8,256,128]{1,2,0:T(8,128)S(1)} fusion(bf16[8,128,128]{2,1,0:T(8,128)(2,1)S(1)} %copy-done, f32[1024]{0:T(1024)S(1)} %select_select_fusion, f32[256]{0:T(256)S(1)} %convert_add_fusion, pred[1024]{0:T(1024)(128)(4,1)S(1)} %get-tuple-element.9, pred[1024]{0:T(1024)(128)(4,1)S(1)} %get-tuple-element.8, ...), kind=kOutput, calls=%fused_computation.23 | convolution fusion | flops 73138176 | bytes 18097152 | tf_op jit(solution)/shard_map/tgc,gcd->tgd/dot_general | solution.py:421
  128.4 2.3 %convolution_convert_fusion = bf16[256,2048]{1,0:T(8,128)(2,1)} fusion(bf16[256,1024]{0,1:T(8,128)(2,1)S(1)} %fusion.3, bf16[1024,2048]{1,0:T(8,128)(2,1)S(1)} %copy-done.8), kind=kOutput, calls=%fused_computation | convolution fusion | flops 1074266112 | bytes 5767168 | tf_op jit(solution)/shard_map/dot_general | solution.py:78
  132.4 16.7 %all-to-all-done.1 = bf16[64,8,768]{2,1,0:T(8,128)(2,1)S(1)} async-done(((bf16[64,8,768]{2,1,0:T(8,128)(2,1)}), bf16[64,8,768]{2,1,0:T(8,128)(2,1)S(1)}, u32[]{:S(2)}, u32[]{:S(2)}) %all-to-all-start.1) | async-done | bytes 786464 | tf_op jit(solution)/shard_map/all_to_all | solution.py:365
  149.2 2.7 %combine.3 = bf16[128,2048]{1,0:T(8,128)(2,1)} custom-call(s32[1]{0:T(128)} %bitcast.2.own_ref, bf16[512,768]{1,0:T(8,128)(2,1)S(1)} %bitcast.40, s32[2,512]{1,0:T(2,128)S(1)} %bitcast.44, f32[2,512]{1,0:T(2,128)S(1)} %bitcast.46, f32[128,2048]{1,0:T(8,128)S(1)} %combine.2.refs_0_), custom_call_target="tpu_custom_call" | custom-call | flops 1500000000 | bytes 2100000 | tf_op jit(solution)/shard_map/combine/pallas_call | solution.py:342
  (49 shorter events, 15.5 us)
Async XLA Ops:
  0.6 125.6 %copy-start = (bf16[8,128,128]{2,1,0:T(8,128)(2,1)S(1)}, bf16[8,128,128]{2,1,0:T(8,128)(2,1)}, u32[]{:S(2)}) copy-start(bf16[8,128,128]{2,1,0:T(8,128)(2,1)} %param.12) | copy-start | bytes 786436
  4.2 36.0 %all-to-all-start.2 = ((bf16[64,8,768]{2,1,0:T(8,128)(2,1)}), bf16[64,8,768]{2,1,0:T(8,128)(2,1)S(1)}, u32[]{:S(2)}, u32[]{:S(2)}) async-start(bf16[64,8,768]{2,1,0:T(8,128)(2,1)} %bitcast.50), calls=%async_computation.2 | async-start | bytes 1572864 | tf_op jit(solution)/shard_map/all_to_all | solution.py:365
  17.2 31.2 %collective-permute-start.1 = (bf16[2048,256]{1,0:T(8,128)(2,1)}, bf16[2048,256]{1,0:T(8,128)(2,1)}, u32[]{:S(2)}, u32[]{:S(2)}) collective-permute-start(bf16[2048,256]{1,0:T(8,128)(2,1)} %bitcast.7.refs_1_), channel_id=1, source_target_pairs={{0,1},{1,0},{2,3},{3,2},{4,7},{5,6},{6,5},{7,4},{8,9},{9,8},{10,11... | collective-permute-start | bytes 3145736 | tf_op jit(solution)/shard_map/ppermute | solution.py:49
  20.0 31.6 %collective-permute-start.2 = (bf16[2048,256]{1,0:T(8,128)(2,1)}, bf16[2048,256]{1,0:T(8,128)(2,1)}, u32[]{:S(2)}, u32[]{:S(2)}) collective-permute-start(bf16[2048,256]{1,0:T(8,128)(2,1)} %bitcast.8.refs_2_), channel_id=1, source_target_pairs={{0,1},{1,0},{2,3},{3,2},{4,7},{5,6},{6,5},{7,4},{8,9},{9,8},{10,11... | collective-permute-start | bytes 3145736 | tf_op jit(solution)/shard_map/ppermute | solution.py:49
  20.1 39.1 %collective-permute-start.3 = (bf16[256,2048]{1,0:T(8,128)(2,1)}, bf16[256,2048]{1,0:T(8,128)(2,1)}, u32[]{:S(2)}, u32[]{:S(2)}) collective-permute-start(bf16[256,2048]{1,0:T(8,128)(2,1)} %bitcast.9.refs_5_), channel_id=1, source_target_pairs={{0,1},{1,0},{2,3},{3,2},{4,7},{5,6},{6,5},{7,4},{8,9},{9,8},{10,11... | collective-permute-start | bytes 3145736 | tf_op jit(solution)/shard_map/ppermute | solution.py:49
  40.2 6.0 %copy-start.4 = (bf16[64,8,768]{2,1,0:T(8,128)(2,1)}, bf16[64,8,768]{2,1,0:T(8,128)(2,1)S(1)}, u32[]{:S(2)}) copy-start(bf16[64,8,768]{2,1,0:T(8,128)(2,1)S(1)} %all-to-all-done.2) | copy-start | bytes 2359300
  40.2 28.9 %all-to-all-start = ((bf16[64,8,768]{2,1,0:T(8,128)(2,1)}), bf16[64,8,768]{2,1,0:T(8,128)(2,1)S(1)}, u32[]{:S(2)}, u32[]{:S(2)}) async-start(bf16[64,8,768]{2,1,0:T(8,128)(2,1)} %bitcast.49), calls=%async_computation | async-start | bytes 1572864 | tf_op jit(solution)/shard_map/all_to_all | solution.py:365
  46.2 13.1 %collective-permute-start.10 = (bf16[256,768]{1,0:T(8,128)(2,1)S(1)}, bf16[256,768]{1,0:T(8,128)(2,1)S(1)}, u32[]{:S(2)}, u32[]{:S(2)}) collective-permute-start(bf16[256,768]{1,0:T(8,128)(2,1)S(1)} %get-tuple-element.2), channel_id=1, source_target_pairs={{0,3},{1,2},{2,1},{3,0},{4,5},{5,4},{6,7},{7,6},{8,11},{9,10},{10,... | collective-permute-start | bytes 1179656 | tf_op jit(solution)/shard_map/ppermute | solution.py:49
  47.6 15.7 %collective-permute-start.8 = (bf16[256,768]{1,0:T(8,128)(2,1)S(1)}, bf16[256,768]{1,0:T(8,128)(2,1)S(1)}, u32[]{:S(2)}, u32[]{:S(2)}) collective-permute-start(bf16[256,768]{1,0:T(8,128)(2,1)S(1)} %get-tuple-element.3), channel_id=1, source_target_pairs={{0,3},{1,2},{2,1},{3,0},{4,5},{5,4},{6,7},{7,6},{8,11},{9,10},{10,... | collective-permute-start | bytes 1179656 | tf_op jit(solution)/shard_map/ppermute | solution.py:49
  48.4 54.6 %collective-permute-start = (bf16[15,1024]{1,0:T(8,128)(2,1)}, bf16[15,1024]{1,0:T(8,128)(2,1)}, u32[]{:S(2)}, u32[]{:S(2)}) collective-permute-start(bf16[15,1024]{1,0:T(8,128)(2,1)} %slice.76), channel_id=1, source_target_pairs={{0,1},{1,2},{2,3},{3,4},{4,5},{5,6},{6,7},{7,8},{8,9},{9,10},{10,1... | collective-permute-start | bytes 92168 | tf_op jit(solution)/shard_map/ppermute | solution.py:39
  62.9 12.3 %collective-permute-start.11 = (bf16[96,2048]{1,0:T(8,128)(2,1)S(1)}, bf16[96,2048]{1,0:T(8,128)(2,1)S(1)}, u32[]{:S(2)}, u32[]{:S(2)}) collective-permute-start(bf16[96,2048]{1,0:T(8,128)(2,1)S(1)} %half_ffn.11), channel_id=1, source_target_pairs={{0,3},{1,2},{2,1},{3,0},{4,5},{5,4},{6,7},{7,6},{8,11},{9,10},{10,... | collective-permute-start | bytes 1179656 | tf_op jit(solution)/shard_map/ppermute | solution.py:49
  66.9 8.3 %collective-permute-start.9 = (bf16[96,2048]{1,0:T(8,128)(2,1)S(1)}, bf16[96,2048]{1,0:T(8,128)(2,1)S(1)}, u32[]{:S(2)}, u32[]{:S(2)}) collective-permute-start(bf16[96,2048]{1,0:T(8,128)(2,1)S(1)} %half_ffn.10), channel_id=1, source_target_pairs={{0,3},{1,2},{2,1},{3,0},{4,5},{5,4},{6,7},{7,6},{8,11},{9,10},{10,... | collective-permute-start | bytes 1179656 | tf_op jit(solution)/shard_map/ppermute | solution.py:49
  69.1 6.0 %copy-start.3 = (bf16[64,8,768]{2,1,0:T(8,128)(2,1)}, bf16[64,8,768]{2,1,0:T(8,128)(2,1)S(1)}, u32[]{:S(2)}) copy-start(bf16[64,8,768]{2,1,0:T(8,128)(2,1)S(1)} %all-to-all-done) | copy-start | bytes 2359300
  70.1 22.3 %collective-permute-start.4 = (bf16[256,768]{1,0:T(8,128)(2,1)}, bf16[256,768]{1,0:T(8,128)(2,1)S(1)}, u32[]{:S(2)}, u32[]{:S(2)}) collective-permute-start(bf16[256,768]{1,0:T(8,128)(2,1)} %get-tuple-element.5), channel_id=1, source_target_pairs={{0,3},{1,2},{2,1},{3,0},{4,5},{5,4},{6,7},{7,6},{8,11},{9,10},{10,... | collective-permute-start | bytes 1179656 | tf_op jit(solution)/shard_map/ppermute | solution.py:49
  77.0 15.4 %copy-start.6 = (bf16[256,768]{1,0:T(8,128)(2,1)S(1)}, bf16[256,768]{1,0:T(8,128)(2,1)}, u32[]{:S(2)}) copy-start(bf16[256,768]{1,0:T(8,128)(2,1)} %get-tuple-element.4) | copy-start | bytes 1179652
  77.0 38.3 %all-to-all-start.3 = ((bf16[64,8,768]{2,1,0:T(8,128)(2,1)}), bf16[64,8,768]{2,1,0:T(8,128)(2,1)S(1)}, u32[]{:S(2)}, u32[]{:S(2)}) async-start(bf16[64,8,768]{2,1,0:T(8,128)(2,1)} %bitcast.19), calls=%async_computation.3 | async-start | bytes 1572864 | tf_op jit(solution)/shard_map/all_to_all | solution.py:365
  92.3 7.0 %collective-permute-start.6 = (bf16[256,768]{1,0:T(8,128)(2,1)S(1)}, bf16[256,768]{1,0:T(8,128)(2,1)S(1)}, u32[]{:S(2)}, u32[]{:S(2)}) collective-permute-start(bf16[256,768]{1,0:T(8,128)(2,1)S(1)} %copy-done.6), channel_id=1, source_target_pairs={{0,3},{1,2},{2,1},{3,0},{4,5},{5,4},{6,7},{7,6},{8,11},{9,10},{10,... | collective-permute-start | bytes 1179656 | tf_op jit(solution)/shard_map/ppermute | solution.py:49
  96.1 11.6 %collective-permute-start.5 = (bf16[96,2048]{1,0:T(8,128)(2,1)S(1)}, bf16[96,2048]{1,0:T(8,128)(2,1)S(1)}, u32[]{:S(2)}, u32[]{:S(2)}) collective-permute-start(bf16[96,2048]{1,0:T(8,128)(2,1)S(1)} %half_ffn.7), channel_id=1, source_target_pairs={{0,3},{1,2},{2,1},{3,0},{4,5},{5,4},{6,7},{7,6},{8,11},{9,10},{10,... | collective-permute-start | bytes 1179656 | tf_op jit(solution)/shard_map/ppermute | solution.py:49
  102.9 7.0 %collective-permute-start.7 = (bf16[96,2048]{1,0:T(8,128)(2,1)S(1)}, bf16[96,2048]{1,0:T(8,128)(2,1)S(1)}, u32[]{:S(2)}, u32[]{:S(2)}) collective-permute-start(bf16[96,2048]{1,0:T(8,128)(2,1)S(1)} %half_ffn.8), channel_id=1, source_target_pairs={{0,3},{1,2},{2,1},{3,0},{4,5},{5,4},{6,7},{7,6},{8,11},{9,10},{10,... | collective-permute-start | bytes 1179656 | tf_op jit(solution)/shard_map/ppermute | solution.py:49
  115.3 33.9 %all-to-all-start.1 = ((bf16[64,8,768]{2,1,0:T(8,128)(2,1)}), bf16[64,8,768]{2,1,0:T(8,128)(2,1)S(1)}, u32[]{:S(2)}, u32[]{:S(2)}) async-start(bf16[64,8,768]{2,1,0:T(8,128)(2,1)} %bitcast.12), calls=%async_computation.1 | async-start | bytes 1572864 | tf_op jit(solution)/shard_map/all_to_all | solution.py:365
  126.2 2.0 %copy-start.7 = (f32[1024]{0:T(1024)S(1)}, f32[1024]{0:T(1024)}, u32[]{:S(2)}) copy-start(f32[1024]{0:T(1024)} %param.13) | copy-start | bytes 12292
  126.2 2.2 %copy-start.8 = (bf16[1024,2048]{1,0:T(8,128)(2,1)S(1)}, bf16[1024,2048]{1,0:T(8,128)(2,1)}, u32[]{:S(2)}) copy-start(bf16[1024,2048]{1,0:T(8,128)(2,1)} %param.14) | copy-start | bytes 12582916
  128.4 2.3 %copy-start.1 = (s32[512,2]{0,1:T(2,128)S(1)}, s32[512,2]{0,1:T(2,128)}, u32[]{:S(2)}) copy-start(s32[512,2]{0,1:T(2,128)} %param.17) | copy-start | bytes 12292
  128.4 2.3 %copy-start.2 = (f32[512,2]{0,1:T(2,128)S(1)}, f32[512,2]{0,1:T(2,128)}, u32[]{:S(2)}) copy-start(f32[512,2]{0,1:T(2,128)} %param.18) | copy-start | bytes 12292
  (1 other events, 1.6 us)
where the time goes:
time: 153 us; the launch traced here: 152 us
  starting transfers between devices  60.2 us (39%)
  waiting for transfers between devices  46.8 us (31%)
  Pallas kernels  36.9 us (24%)
  matrix products  4.18 us (3%)
  local copies, waits for them, and re-layouts  1.75 us (1%)
    all_to_all x4, starting transfers between devices, exchanged(): lax.all_to_all(rows.reshape(experts, SUB, LANES), 'ep', split_axis=0, con...  45.1 us
    all_to_all x4, waiting for transfers between devices, exchanged(): lax.all_to_all(rows.reshape(experts, SUB, LANES), 'ep', split_axis=0, con...  34.8 us
    pallas_call x6, Pallas kernels, half_ffn(): pl.pallas_call(ffn_kernel, out_shape=jax.ShapeDtypeStruct((dense, WIDTH),...  21.8 us
    ppermute x11, waiting for transfers between devices, swapped(): return lax.ppermute(array, ('ep', 'tp'), pairs)  12 us
    ppermute x11, starting transfers between devices, swapped(): return lax.ppermute(array, ('ep', 'tp'), pairs)  11.9 us
    pallas_call x2, Pallas kernels, send_rows(): pl.pallas_call(partial(send_kernel, chunk * SLOTS), out_shape=jax.ShapeDt...  7.05 us
    pallas_call x2, Pallas kernels, combine(): pl.pallas_call(partial(combine_kernel, chunk * SLOTS), out_shape=jax.Shap...  4.51 us
    pallas_call x2, Pallas kernels, pack_sum(): pl.pallas_call(pack_kernel, out_shape=jax.ShapeDtypeStruct((rows, LANES),...  3.59 us
  transfers between devices with their start and end apart: 16, of which 8 were waited for; matrix products, arithmetic and copies ran while one was open for 5% of the time, Pallas kernels for 20%

commit v1 on v0

--- a/solution.py
+++ b/solution.py
@@ -26,7 +26,6 @@
 DENSE = EXPERTS_G * SLOTS
 SMALL = 16 * 1024 * 1024
 LARGE = 52 * 1024 * 1024
-LARGER = 53 * 1024 * 1024
 BF16 = jnp.bfloat16
 F32 = jnp.float32
 VMEM = pl.BlockSpec(memory_space=pltpu.VMEM)
@@ -204,37 +203,37 @@
         put(block, g, start)
 
 
-def pack_kernel(a_ref, *refs):
-    *b_refs, out_ref = refs
+def pack_kernel(a_ref, b_ref, out_ref):
     experts = out_ref.shape[0] // SUB
     mains = main_maps((GROUP, DENSE), 1)
     for c in range(FOLD):
         maps = jnp.concatenate(mains + tail_maps((GROUP, DENSE), 1, c), axis=1)
-        for g, b_ref in enumerate(b_refs):
+        for g in range(experts // EXPERTS_G):
             pieces = []
             for start in dense_columns(c):
                 columns = slice(start, start + PIECE)
                 for k in range(SLOTS):
-                    at = k * experts + g * EXPERTS_G
-                    own = a_ref[at : at + EXPERTS_G, columns].astype(F32)
-                    other = b_ref[k * EXPERTS_G : (k + 1) * EXPERTS_G, columns].astype(F32)
-                    pieces.append((own + other).astype(BF16))
+                    to = k * experts + g * EXPERTS_G
+                    here = slice(to, to + EXPERTS_G)
+                    pieces.append(
+                        (a_ref[here, columns].astype(F32) + b_ref[here, columns].astype(F32)).astype(BF16)
+                    )
             out_ref[g * GROUP : (g + 1) * GROUP, c * PIECE : (c + 1) * PIECE] = dot(
                 maps, jnp.concatenate(pieces, axis=0)
             ).astype(BF16)
 
 
-def pack_sum(a, parts):
+def pack_sum(a, b):
     rows = a.shape[0] // SLOTS * SUB
     return pl.pallas_call(
         pack_kernel,
         out_shape=jax.ShapeDtypeStruct((rows, LANES), BF16),
-        in_specs=[VMEM] * (1 + len(parts)),
+        in_specs=[VMEM] * 2,
         out_specs=VMEM,
         cost_estimate=pl.CostEstimate(flops=800_000_000, bytes_accessed=a.size * 6, transcendentals=0),
         compiler_params=pltpu.CompilerParams(vmem_limit_bytes=SMALL),
         name="pack_sum",
-    )(a, *parts)
+    )(a, b)
 
 
 def ffn_kernel(*refs):
@@ -283,7 +282,7 @@
             bytes_accessed=x.size * 4 + 6 * ga.size * 2,
             transcendentals=dense * hidden,
         ),
-        compiler_params=pltpu.CompilerParams(vmem_limit_bytes=LARGER),
+        compiler_params=pltpu.CompilerParams(vmem_limit_bytes=LARGE),
         name="half_ffn",
     )(*operands)
 
@@ -399,14 +398,9 @@
         mine.append(exchanged(sent))
     expert_out = None
     for n in range(CHUNKS):
-        back = []
-        halves = mine[n].shape[0] // GROUP
-        theirs = []
-        for g in range(halves):
-            theirs.append(swapped(mine[n][g * GROUP : (g + 1) * GROUP], 1))
-        for g in range(halves):
-            partial_sum = ffn(theirs[g])
-            back.append(swapped(partial_sum, 1))
+        theirs = swapped(mine[n], 1)
+        partial_sum = ffn(theirs)
+        back = swapped(partial_sum, 1)
         kept = ffn(mine[n])
         results = pack_sum(kept, back)
         returned = exchanged(results)

time: 153 us -> 157 us (1.026)
  waiting for transfers between devices: 46.8 us -> 63.5 us
  Pallas kernels: 36.9 us -> 30.2 us
  starting transfers between devices: 60.2 us -> 56.9 us
  local copies, waits for them, and re-layouts: 1.75 us -> 0.07 us
    ppermute x11 -> x7, waiting for transfers between devices: 12 us -> 26.1 us  [swapped(): return lax.ppermute(array, ('ep', 'tp'), pairs)]
    pallas_call x6 -> x4, Pallas kernels: 21.8 us -> 14 us  [half_ffn(): pl.pallas_call(ffn_kernel, out_shape=jax.ShapeDtypeStruct((dense, WIDTH),...]
    ppermute x11 -> x7, starting transfers between devices: 11.9 us -> 9.73 us  [swapped(): return lax.ppermute(array, ('ep', 'tp'), pairs)]
  transfers between devices with their start and end apart: 16 -> 12, of which waited for: 8 -> 9; matrix products, arithmetic and copies ran while one was open for 5% -> 3% of each run, Pallas kernels for 20% -> 15%
where the time goes in v1:
time: 157 us; the launch traced here: 156 us
  waiting for transfers between devices  63.5 us (40%)
  starting transfers between devices  56.9 us (36%)
  Pallas kernels  30.2 us (19%)
  matrix products  4.18 us (3%)
    all_to_all x4, starting transfers between devices, exchanged(): lax.all_to_all(rows.reshape(experts, SUB, LANES), 'ep', split_axis=0, con...  45.2 us
    all_to_all x4, waiting for transfers between devices, exchanged(): lax.all_to_all(rows.reshape(experts, SUB, LANES), 'ep', split_axis=0, con...  36.2 us
    ppermute x7, waiting for transfers between devices, swapped(): return lax.ppermute(array, ('ep', 'tp'), pairs)  26.1 us
    pallas_call x4, Pallas kernels, half_ffn(): pl.pallas_call(ffn_kernel, out_shape=jax.ShapeDtypeStruct((dense, WIDTH),...  14 us
    ppermute x7, starting transfers between devices, swapped(): return lax.ppermute(array, ('ep', 'tp'), pairs)  9.73 us
    pallas_call x2, Pallas kernels, send_rows(): pl.pallas_call(partial(send_kernel, chunk * SLOTS), out_shape=jax.ShapeDt...  7.05 us
    pallas_call x2, Pallas kernels, pack_sum(): pl.pallas_call(pack_kernel, out_shape=jax.ShapeDtypeStruct((rows, LANES),...  4.67 us
    pallas_call x2, Pallas kernels, combine(): pl.pallas_call(partial(combine_kernel, chunk * SLOTS), out_shape=jax.Shap...  4.51 us
  transfers between devices with their start and end apart: 12, of which 9 were waited for; matrix products, arithmetic and copies ran while one was open for 3% of the time, Pallas kernels for 15%

profile of v1, /device:TPU:1, one launch (start us, length us, event | category | flops | bytes accessed | tf_op | source)
XLA Modules:
  0.0 156.3 jit_solution(6130007810891531162)
XLA Ops:
  0.6 3.5 %send_rows.3 = bf16[512,768]{1,0:T(8,128)(2,1)} custom-call(s32[1]{0:T(128)} %bitcast.2.own_ref, bf16[512,2048]{1,0:T(8,128)(2,1)} %rows_hbm.3, f32[1,2048]{1,0:T(1,128)} %bitcast.45, s32[2,512]{1,0:T(2,128)} %bitcast.37), custom_call_target="tpu_custom_call" | custom-call | flops 2000000000 | bytes 2100000 | tf_op jit(solution)/shard_map/send_rows/pallas_call | solution.py:138
  4.2 13.0 %all-to-all-start.2 = ((bf16[64,8,768]{2,1,0:T(8,128)(2,1)}), bf16[64,8,768]{2,1,0:T(8,128)(2,1)S(1)}, u32[]{:S(2)}, u32[]{:S(2)}) async-start(bf16[64,8,768]{2,1,0:T(8,128)(2,1)} %bitcast.44), calls=%async_computation.2 | async-start | bytes 1572864 | tf_op jit(solution)/shard_map/all_to_all | solution.py:364
  17.2 2.8 %collective-permute-start.1 = (bf16[2048,256]{1,0:T(8,128)(2,1)}, bf16[2048,256]{1,0:T(8,128)(2,1)}, u32[]{:S(2)}, u32[]{:S(2)}) collective-permute-start(bf16[2048,256]{1,0:T(8,128)(2,1)} %bitcast.7.refs_1_), channel_id=1, source_target_pairs={{0,1},{1,0},{2,3},{3,2},{4,7},{5,6},{6,5},{7,4},{8,9},{9,8},{10,11... | collective-permute-start | bytes 3145736 | tf_op jit(solution)/shard_map/ppermute | solution.py:48
  20.1 2.6 %collective-permute-start.3 = (bf16[256,2048]{1,0:T(8,128)(2,1)}, bf16[256,2048]{1,0:T(8,128)(2,1)}, u32[]{:S(2)}, u32[]{:S(2)}) collective-permute-start(bf16[256,2048]{1,0:T(8,128)(2,1)} %bitcast.9.refs_5_), channel_id=1, source_target_pairs={{0,1},{1,0},{2,3},{3,2},{4,7},{5,6},{6,5},{7,4},{8,9},{9,8},{10,11... | collective-permute-start | bytes 3145736 | tf_op jit(solution)/shard_map/ppermute | solution.py:48
  22.7 3.5 %send_rows.2 = bf16[512,768]{1,0:T(8,128)(2,1)} custom-call(s32[1]{0:T(128)} %bitcast.2.own_ref, bf16[512,2048]{1,0:T(8,128)(2,1)} %rows_hbm.3, f32[1,2048]{1,0:T(1,128)} %bitcast.46, s32[2,512]{1,0:T(2,128)} %bitcast.38), custom_call_target="tpu_custom_call" | custom-call | flops 2000000000 | bytes 2100000 | tf_op jit(solution)/shard_map/send_rows/pallas_call | solution.py:138
  26.2 14.0 %all-to-all-done.2 = bf16[64,8,768]{2,1,0:T(8,128)(2,1)S(1)} async-done(((bf16[64,8,768]{2,1,0:T(8,128)(2,1)}), bf16[64,8,768]{2,1,0:T(8,128)(2,1)S(1)}, u32[]{:S(2)}, u32[]{:S(2)}) %all-to-all-start.2) | async-done | bytes 786464 | tf_op jit(solution)/shard_map/all_to_all | solution.py:364
  40.2 5.9 %all-to-all-start = ((bf16[64,8,768]{2,1,0:T(8,128)(2,1)}), bf16[64,8,768]{2,1,0:T(8,128)(2,1)S(1)}, u32[]{:S(2)}, u32[]{:S(2)}) async-start(bf16[64,8,768]{2,1,0:T(8,128)(2,1)} %bitcast.43), calls=%async_computation | async-start | bytes 1572864 | tf_op jit(solution)/shard_map/all_to_all | solution.py:364
  47.5 11.8 %collective-permute-done.3.refs_6_ = bf16[256,2048]{1,0:T(8,128)(2,1)} collective-permute-done((bf16[256,2048]{1,0:T(8,128)(2,1)}, bf16[256,2048]{1,0:T(8,128)(2,1)}, u32[]{:S(2)}, u32[]{:S(2)}) %collective-permute-start.3) | collective-permute-done | bytes 1048608 | tf_op jit(solution)/shard_map/ppermute | solution.py:48
  59.3 3.9 %collective-permute-done.6.refs_0_ = bf16[512,768]{1,0:T(8,128)(2,1)S(1)} collective-permute-done((bf16[512,768]{1,0:T(8,128)(2,1)S(1)}, bf16[512,768]{1,0:T(8,128)(2,1)S(1)}, u32[]{:S(2)}, u32[]{:S(2)}) %collective-permute-start.6) | collective-permute-done | bytes 786464 | tf_op jit(solution)/shard_map/ppermute | solution.py:48
  63.3 3.5 %half_ffn.7 = bf16[192,2048]{1,0:T(8,128)(2,1)S(1)} custom-call(bf16[512,768]{1,0:T(8,128)(2,1)S(1)} %collective-permute-done.6.refs_0_, bf16[2048,256]{1,0:T(8,128)(2,1)} %bitcast.7.refs_1_, bf16[2048,256]{1,0:T(8,128)(2,1)} %bitcast.8.refs_2_, bf16[2048,256]{1,0:T(8,128)(2,1)} %collective-permute-done.1.refs_3_, ...), custom_call_target="tpu_custom_call" | custom-call | flops 3500000000 | bytes 7864320 | tf_op jit(solution)/shard_map/half_ffn/pallas_call | solution.py:272
  70.4 3.5 %half_ffn.6.a_ref = bf16[192,2048]{1,0:T(8,128)(2,1)S(1)} custom-call(bf16[512,768]{1,0:T(8,128)(2,1)S(1)} %bitcast.35, bf16[2048,256]{1,0:T(8,128)(2,1)} %bitcast.7.refs_1_, bf16[2048,256]{1,0:T(8,128)(2,1)} %bitcast.8.refs_2_, bf16[2048,256]{1,0:T(8,128)(2,1)} %collective-permute-done.1.refs_3_, bf16[2048,256]{1,0:T(8,128)(2,1)} %collective-permute-done.2.refs_4_, ...), custom_call_target="tpu_custom_call" | custom-call | flops 3500000000 | bytes 7864320 | tf_op jit(solution)/shard_map/half_ffn/pallas_call | solution.py:272
  73.9 4.2 %collective-permute-done.7.b_ref = bf16[192,2048]{1,0:T(8,128)(2,1)} collective-permute-done((bf16[192,2048]{1,0:T(8,128)(2,1)S(1)}, bf16[192,2048]{1,0:T(8,128)(2,1)}, u32[]{:S(2)}, u32[]{:S(2)}) %collective-permute-start.7) | collective-permute-done | bytes 786464 | tf_op jit(solution)/shard_map/ppermute | solution.py:48
  78.1 2.9 %pack_sum.3 = bf16[512,768]{1,0:T(8,128)(2,1)} custom-call(bf16[192,2048]{1,0:T(8,128)(2,1)S(1)} %half_ffn.6.a_ref, bf16[192,2048]{1,0:T(8,128)(2,1)} %collective-permute-done.7.b_ref), custom_call_target="tpu_custom_call" | custom-call | flops 800000000 | bytes 2359296 | tf_op jit(solution)/shard_map/pack_sum/pallas_call | solution.py:228
  81.0 12.9 %all-to-all-start.3 = ((bf16[64,8,768]{2,1,0:T(8,128)(2,1)}), bf16[64,8,768]{2,1,0:T(8,128)(2,1)S(1)}, u32[]{:S(2)}, u32[]{:S(2)}) async-start(bf16[64,8,768]{2,1,0:T(8,128)(2,1)} %bitcast.15), calls=%async_computation.3 | async-start | bytes 1572864 | tf_op jit(solution)/shard_map/all_to_all | solution.py:364
  93.9 1.9 %collective-permute-start = (bf16[15,1024]{1,0:T(8,128)(2,1)S(1)}, bf16[15,1024]{1,0:T(8,128)(2,1)S(1)}, u32[]{:S(2)}, u32[]{:S(2)}) collective-permute-start(bf16[15,1024]{1,0:T(8,128)(2,1)S(1)} %slice.52), channel_id=1, source_target_pairs={{0,1},{1,2},{2,3},{3,4},{4,5},{5,6},{6,7},{7,8},{8,9},{9,10},{10,1... | collective-permute-start | bytes 92168 | tf_op jit(solution)/shard_map/ppermute | solution.py:38
  95.9 3.5 %half_ffn.5 = bf16[192,2048]{1,0:T(8,128)(2,1)S(1)} custom-call(bf16[512,768]{1,0:T(8,128)(2,1)S(1)} %collective-permute-done.4.refs_0_, bf16[2048,256]{1,0:T(8,128)(2,1)} %bitcast.7.refs_1_, bf16[2048,256]{1,0:T(8,128)(2,1)} %bitcast.8.refs_2_, bf16[2048,256]{1,0:T(8,128)(2,1)} %collective-permute-done.1.refs_3_, ...), custom_call_target="tpu_custom_call" | custom-call | flops 3500000000 | bytes 7864320 | tf_op jit(solution)/shard_map/half_ffn/pallas_call | solution.py:272
  100.9 3.5 %half_ffn.4.a_ref = bf16[192,2048]{1,0:T(8,128)(2,1)S(1)} custom-call(bf16[512,768]{1,0:T(8,128)(2,1)S(1)} %bitcast.32, bf16[2048,256]{1,0:T(8,128)(2,1)} %bitcast.7.refs_1_, bf16[2048,256]{1,0:T(8,128)(2,1)} %bitcast.8.refs_2_, bf16[2048,256]{1,0:T(8,128)(2,1)} %collective-permute-done.1.refs_3_, bf16[2048,256]{1,0:T(8,128)(2,1)} %collective-permute-done.2.refs_4_, ...), custom_call_target="tpu_custom_call" | custom-call | flops 3500000000 | bytes 7864320 | tf_op jit(solution)/shard_map/half_ffn/pallas_call | solution.py:272
  104.4 6.2 %collective-permute-done.5.b_ref = bf16[192,2048]{1,0:T(8,128)(2,1)S(1)} collective-permute-done((bf16[192,2048]{1,0:T(8,128)(2,1)S(1)}, bf16[192,2048]{1,0:T(8,128)(2,1)S(1)}, u32[]{:S(2)}, u32[]{:S(2)}) %collective-permute-start.5) | collective-permute-done | bytes 786464 | tf_op jit(solution)/shard_map/ppermute | solution.py:48
  112.4 4.5 %all-to-all-done.3 = bf16[64,8,768]{2,1,0:T(8,128)(2,1)S(1)} async-done(((bf16[64,8,768]{2,1,0:T(8,128)(2,1)}), bf16[64,8,768]{2,1,0:T(8,128)(2,1)S(1)}, u32[]{:S(2)}, u32[]{:S(2)}) %all-to-all-start.3) | async-done | bytes 786464 | tf_op jit(solution)/shard_map/all_to_all | solution.py:364
  116.9 13.5 %all-to-all-start.1 = ((bf16[64,8,768]{2,1,0:T(8,128)(2,1)}), bf16[64,8,768]{2,1,0:T(8,128)(2,1)S(1)}, u32[]{:S(2)}, u32[]{:S(2)}) async-start(bf16[64,8,768]{2,1,0:T(8,128)(2,1)} %bitcast.10), calls=%async_computation.1 | async-start | bytes 1572864 | tf_op jit(solution)/shard_map/all_to_all | solution.py:364
  130.4 1.9 %fusion.5 = f32[8,256,128]{1,2,0:T(8,128)S(1)} fusion(bf16[8,128,128]{2,1,0:T(8,128)(2,1)S(1)} %copy-done, f32[1024]{0:T(1024)S(1)} %select_select_fusion, f32[256]{0:T(256)S(1)} %convert_add_fusion, pred[1024]{0:T(1024)(128)(4,1)S(1)} %get-tuple-element.5, pred[1024]{0:T(1024)(128)(4,1)S(1)} %get-tuple-element.4, ...), kind=kOutput, calls=%fused_computation.23 | convolution fusion | flops 73138176 | bytes 18097152 | tf_op jit(solution)/shard_map/tgc,gcd->tgd/dot_general | solution.py:415
  132.6 2.2 %convolution_convert_fusion = bf16[256,2048]{1,0:T(8,128)(2,1)} fusion(bf16[256,1024]{0,1:T(8,128)(2,1)S(1)} %fusion.3, bf16[1024,2048]{1,0:T(8,128)(2,1)S(1)} %copy-done.5), kind=kOutput, calls=%fused_computation | convolution fusion | flops 1074266112 | bytes 5767168 | tf_op jit(solution)/shard_map/dot_general | solution.py:77
  136.6 16.7 %all-to-all-done.1 = bf16[64,8,768]{2,1,0:T(8,128)(2,1)S(1)} async-done(((bf16[64,8,768]{2,1,0:T(8,128)(2,1)}), bf16[64,8,768]{2,1,0:T(8,128)(2,1)S(1)}, u32[]{:S(2)}, u32[]{:S(2)}) %all-to-all-start.1) | async-done | bytes 786464 | tf_op jit(solution)/shard_map/all_to_all | solution.py:364
  153.3 2.7 %combine.3 = bf16[128,2048]{1,0:T(8,128)(2,1)} custom-call(s32[1]{0:T(128)} %bitcast.2.own_ref, bf16[512,768]{1,0:T(8,128)(2,1)S(1)} %bitcast.36, s32[2,512]{1,0:T(2,128)S(1)} %bitcast.40, f32[2,512]{1,0:T(2,128)S(1)} %bitcast.42, f32[128,2048]{1,0:T(8,128)S(1)} %combine.2.refs_0_), custom_call_target="tpu_custom_call" | custom-call | flops 1500000000 | bytes 2100000 | tf_op jit(solution)/shard_map/combine/pallas_call | solution.py:341
  (31 shorter events, 10.4 us)
Async XLA Ops:
  0.6 129.7 %copy-start = (bf16[8,128,128]{2,1,0:T(8,128)(2,1)S(1)}, bf16[8,128,128]{2,1,0:T(8,128)(2,1)}, u32[]{:S(2)}) copy-start(bf16[8,128,128]{2,1,0:T(8,128)(2,1)} %param.12) | copy-start | bytes 786436
  4.2 36.0 %all-to-all-start.2 = ((bf16[64,8,768]{2,1,0:T(8,128)(2,1)}), bf16[64,8,768]{2,1,0:T(8,128)(2,1)S(1)}, u32[]{:S(2)}, u32[]{:S(2)}) async-start(bf16[64,8,768]{2,1,0:T(8,128)(2,1)} %bitcast.44), calls=%async_computation.2 | async-start | bytes 1572864 | tf_op jit(solution)/shard_map/all_to_all | solution.py:364
  17.2 30.3 %collective-permute-start.1 = (bf16[2048,256]{1,0:T(8,128)(2,1)}, bf16[2048,256]{1,0:T(8,128)(2,1)}, u32[]{:S(2)}, u32[]{:S(2)}) collective-permute-start(bf16[2048,256]{1,0:T(8,128)(2,1)} %bitcast.7.refs_1_), channel_id=1, source_target_pairs={{0,1},{1,0},{2,3},{3,2},{4,7},{5,6},{6,5},{7,4},{8,9},{9,8},{10,11... | collective-permute-start | bytes 3145736 | tf_op jit(solution)/shard_map/ppermute | solution.py:48
  20.0 27.5 %collective-permute-start.2 = (bf16[2048,256]{1,0:T(8,128)(2,1)}, bf16[2048,256]{1,0:T(8,128)(2,1)}, u32[]{:S(2)}, u32[]{:S(2)}) collective-permute-start(bf16[2048,256]{1,0:T(8,128)(2,1)} %bitcast.8.refs_2_), channel_id=1, source_target_pairs={{0,1},{1,0},{2,3},{3,2},{4,7},{5,6},{6,5},{7,4},{8,9},{9,8},{10,11... | collective-permute-start | bytes 3145736 | tf_op jit(solution)/shard_map/ppermute | solution.py:48
  20.1 39.2 %collective-permute-start.3 = (bf16[256,2048]{1,0:T(8,128)(2,1)}, bf16[256,2048]{1,0:T(8,128)(2,1)}, u32[]{:S(2)}, u32[]{:S(2)}) collective-permute-start(bf16[256,2048]{1,0:T(8,128)(2,1)} %bitcast.9.refs_5_), channel_id=1, source_target_pairs={{0,1},{1,0},{2,3},{3,2},{4,7},{5,6},{6,5},{7,4},{8,9},{9,8},{10,11... | collective-permute-start | bytes 3145736 | tf_op jit(solution)/shard_map/ppermute | solution.py:48
  40.2 28.9 %all-to-all-start = ((bf16[64,8,768]{2,1,0:T(8,128)(2,1)}), bf16[64,8,768]{2,1,0:T(8,128)(2,1)S(1)}, u32[]{:S(2)}, u32[]{:S(2)}) async-start(bf16[64,8,768]{2,1,0:T(8,128)(2,1)} %bitcast.43), calls=%async_computation | async-start | bytes 1572864 | tf_op jit(solution)/shard_map/all_to_all | solution.py:364
  46.1 17.1 %collective-permute-start.6 = (bf16[512,768]{1,0:T(8,128)(2,1)S(1)}, bf16[512,768]{1,0:T(8,128)(2,1)S(1)}, u32[]{:S(2)}, u32[]{:S(2)}) collective-permute-start(bf16[512,768]{1,0:T(8,128)(2,1)S(1)} %bitcast.34), channel_id=1, source_target_pairs={{0,3},{1,2},{2,1},{3,0},{4,5},{5,4},{6,7},{7,6},{8,11},{9,10},{10,... | collective-permute-start | bytes 2359304 | tf_op jit(solution)/shard_map/ppermute | solution.py:48
  66.8 11.3 %collective-permute-start.7 = (bf16[192,2048]{1,0:T(8,128)(2,1)S(1)}, bf16[192,2048]{1,0:T(8,128)(2,1)}, u32[]{:S(2)}, u32[]{:S(2)}) collective-permute-start(bf16[192,2048]{1,0:T(8,128)(2,1)S(1)} %half_ffn.7), channel_id=1, source_target_pairs={{0,3},{1,2},{2,1},{3,0},{4,5},{5,4},{6,7},{7,6},{8,11},{9,10},{10,... | collective-permute-start | bytes 2359304 | tf_op jit(solution)/shard_map/ppermute | solution.py:48
  69.1 26.7 %collective-permute-start.4 = (bf16[512,768]{1,0:T(8,128)(2,1)S(1)}, bf16[512,768]{1,0:T(8,128)(2,1)S(1)}, u32[]{:S(2)}, u32[]{:S(2)}) collective-permute-start(bf16[512,768]{1,0:T(8,128)(2,1)S(1)} %bitcast.31), channel_id=1, source_target_pairs={{0,3},{1,2},{2,1},{3,0},{4,5},{5,4},{6,7},{7,6},{8,11},{9,10},{10,... | collective-permute-start | bytes 2359304 | tf_op jit(solution)/shard_map/ppermute | solution.py:48
  81.0 12.9 %copy-start.3 = (bf16[256,1024]{1,0:T(8,128)(2,1)S(1)}, bf16[256,1024]{1,0:T(8,128)(2,1)}, u32[]{:S(2)}) copy-start(bf16[256,1024]{1,0:T(8,128)(2,1)} %param.11) | copy-start | bytes 1572868
  81.0 35.9 %all-to-all-start.3 = ((bf16[64,8,768]{2,1,0:T(8,128)(2,1)}), bf16[64,8,768]{2,1,0:T(8,128)(2,1)S(1)}, u32[]{:S(2)}, u32[]{:S(2)}) async-start(bf16[64,8,768]{2,1,0:T(8,128)(2,1)} %bitcast.15), calls=%async_computation.3 | async-start | bytes 1572864 | tf_op jit(solution)/shard_map/all_to_all | solution.py:364
  93.9 6.8 %collective-permute-start = (bf16[15,1024]{1,0:T(8,128)(2,1)S(1)}, bf16[15,1024]{1,0:T(8,128)(2,1)S(1)}, u32[]{:S(2)}, u32[]{:S(2)}) collective-permute-start(bf16[15,1024]{1,0:T(8,128)(2,1)S(1)} %slice.52), channel_id=1, source_target_pairs={{0,1},{1,2},{2,3},{3,4},{4,5},{5,6},{6,7},{7,8},{8,9},{9,10},{10,1... | collective-permute-start | bytes 92168 | tf_op jit(solution)/shard_map/ppermute | solution.py:38
  99.4 11.2 %collective-permute-start.5 = (bf16[192,2048]{1,0:T(8,128)(2,1)S(1)}, bf16[192,2048]{1,0:T(8,128)(2,1)S(1)}, u32[]{:S(2)}, u32[]{:S(2)}) collective-permute-start(bf16[192,2048]{1,0:T(8,128)(2,1)S(1)} %half_ffn.5), channel_id=1, source_target_pairs={{0,3},{1,2},{2,1},{3,0},{4,5},{5,4},{6,7},{7,6},{8,11},{9,10},{10,... | collective-permute-start | bytes 2359304 | tf_op jit(solution)/shard_map/ppermute | solution.py:48
  116.9 36.5 %all-to-all-start.1 = ((bf16[64,8,768]{2,1,0:T(8,128)(2,1)}), bf16[64,8,768]{2,1,0:T(8,128)(2,1)S(1)}, u32[]{:S(2)}, u32[]{:S(2)}) async-start(bf16[64,8,768]{2,1,0:T(8,128)(2,1)} %bitcast.10), calls=%async_computation.1 | async-start | bytes 1572864 | tf_op jit(solution)/shard_map/all_to_all | solution.py:364
  130.3 2.0 %copy-start.4 = (f32[1024]{0:T(1024)S(1)}, f32[1024]{0:T(1024)}, u32[]{:S(2)}) copy-start(f32[1024]{0:T(1024)} %param.13) | copy-start | bytes 12292
  130.4 2.2 %copy-start.5 = (bf16[1024,2048]{1,0:T(8,128)(2,1)S(1)}, bf16[1024,2048]{1,0:T(8,128)(2,1)}, u32[]{:S(2)}) copy-start(bf16[1024,2048]{1,0:T(8,128)(2,1)} %param.14) | copy-start | bytes 12582916
  132.6 2.3 %copy-start.1 = (s32[512,2]{0,1:T(2,128)S(1)}, s32[512,2]{0,1:T(2,128)}, u32[]{:S(2)}) copy-start(s32[512,2]{0,1:T(2,128)} %param.17) | copy-start | bytes 12292
  132.6 2.3 %copy-start.2 = (f32[512,2]{0,1:T(2,128)S(1)}, f32[512,2]{0,1:T(2,128)}, u32[]{:S(2)}) copy-start(f32[512,2]{0,1:T(2,128)} %param.18) | copy-start | bytes 12292

commit v2 on v1

--- a/solution.py
+++ b/solution.py
@@ -102,26 +102,49 @@
     return any((r * FOLD + c - piece) % 2 == 0 for r in range(SUB - 2 * SLOTS))
 
 
-def send_kernel(base, own_ref, rows_hbm, gain_ref, routes_ref, out_ref, rows_ref, normed_ref, sems):
+def send_kernel(
+    base,
+    own_ref,
+    rows_hbm,
+    gain_hbm,
+    routes_hbm,
+    out_hbm,
+    rows_ref,
+    normed_ref,
+    gain_ref,
+    routes_ref,
+    out_ref,
+    sems,
+    out_sems,
+):
     tokens = rows_ref.shape[0]
     half = tokens // 2
-    copies = []
-    for n in range(2):
-        here = pl.ds(pl.multiple_of(own_ref[0] * tokens + n * half, half), half)
-        copies.append(
-            pltpu.make_async_copy(
-                rows_hbm.at[here], rows_ref.at[pl.ds(n * half, half)], sems.at[n]
-            )
+    first = pl.multiple_of(own_ref[0] * tokens, tokens)
+    fetches = [
+        pltpu.make_async_copy(routes_hbm.at[:, pl.ds(first, tokens)], routes_ref, sems.at[2]),
+        pltpu.make_async_copy(gain_hbm, gain_ref, sems.at[3]),
+    ]
+    halves = [
+        pltpu.make_async_copy(
+            rows_hbm.at[pl.ds(pl.multiple_of(first + n * half, half), half)],
+            rows_ref.at[pl.ds(n * half, half)],
+            sems.at[n],
         )
-        copies[n].start()
+        for n in range(2)
+    ]
+    for copy in fetches + halves:
+        copy.start()
+    fetches[0].wait()
     _, named, rank, sub = slot_ranks(routes_ref, out_ref.shape[0], tokens, base)
     mains = jnp.concatenate([as_bf16(named & main_place(sub, rank, h)) for h in range(2)], axis=1)
+    fetches[1].wait()
     for n in range(2):
         here = slice(n * half, (n + 1) * half)
-        copies[n].wait()
+        halves[n].wait()
         features = rows_ref[here, :].astype(F32)
         inverse = lax.rsqrt(jnp.mean(features * features, axis=-1, keepdims=True) + EPS)
         normed_ref[here, :] = (features * inverse * gain_ref[...]).astype(BF16)
+    outs = []
     for c in range(FOLD):
         used = [u for u in range(2) if tail_used(u, c)]
         tails = [as_bf16(named & tail_place(sub, rank, u, c)) for u in used]
@@ -130,6 +153,15 @@
             jnp.concatenate([mains, *tails], axis=1),
             jnp.concatenate([normed_ref[:, start : start + PIECE] for start in starts], axis=0),
         ).astype(BF16)
+        outs.append(column_copy(out_ref, out_hbm, c * PIECE, PIECE, out_sems.at[c]))
+        outs[-1].start()
+    for copy in outs:
+        copy.wait()
+
+
+def column_copy(source, target, at, width, sem):
+    columns = pl.ds(at, width)
+    return pltpu.make_async_copy(source.at[:, columns], target.at[:, columns], sem)
 
 
 def send_rows(expert_in, gain, routes_t, own, experts, chunk):
@@ -141,13 +173,17 @@
         grid_spec=pltpu.PrefetchScalarGridSpec(
             num_scalar_prefetch=1,
             grid=(1,),
-            in_specs=[
-                ANY,
-                pl.BlockSpec((1, width), lambda i, own: (0, 0)),
-                pl.BlockSpec((K, tokens), lambda i, own: (0, own[0])),
+            in_specs=[ANY] * 3,
+            out_specs=ANY,
+            scratch_shapes=[
+                pltpu.VMEM((tokens, width), BF16),
+                pltpu.VMEM((tokens, width), BF16),
+                pltpu.VMEM((1, width), F32),
+                pltpu.VMEM((K, tokens), jnp.int32),
+                pltpu.VMEM((experts * SUB, LANES), BF16),
+                pltpu.SemaphoreType.DMA((4,)),
+                pltpu.SemaphoreType.DMA((FOLD,)),
             ],
-            out_specs=VMEM,
-            scratch_shapes=[pltpu.VMEM((tokens, width), BF16)] * 2 + [pltpu.SemaphoreType.DMA((2,))],
         ),
         cost_estimate=pl.CostEstimate(flops=2_000_000_000, bytes_accessed=2_100_000, transcendentals=128),
         name="send_rows",
@@ -203,7 +239,8 @@
         put(block, g, start)
 
 
-def pack_kernel(a_ref, b_ref, out_ref):
+def pack_kernel(a_ref, b_ref, out_hbm, out_ref, sems):
+    copies = []
     experts = out_ref.shape[0] // SUB
     mains = main_maps((GROUP, DENSE), 1)
     for c in range(FOLD):
@@ -221,6 +258,10 @@
             out_ref[g * GROUP : (g + 1) * GROUP, c * PIECE : (c + 1) * PIECE] = dot(
                 maps, jnp.concatenate(pieces, axis=0)
             ).astype(BF16)
+        copies.append(column_copy(out_ref, out_hbm, c * PIECE, PIECE, sems.at[c]))
+        copies[-1].start()
+    for copy in copies:
+        copy.wait()
 
 
 def pack_sum(a, b):
@@ -229,7 +270,8 @@
         pack_kernel,
         out_shape=jax.ShapeDtypeStruct((rows, LANES), BF16),
         in_specs=[VMEM] * 2,
-        out_specs=VMEM,
+        out_specs=ANY,
+        scratch_shapes=[pltpu.VMEM((rows, LANES), BF16), pltpu.SemaphoreType.DMA((FOLD,))],
         cost_estimate=pl.CostEstimate(flops=800_000_000, bytes_accessed=a.size * 6, transcendentals=0),
         compiler_params=pltpu.CompilerParams(vmem_limit_bytes=SMALL),
         name="pack_sum",
@@ -243,10 +285,12 @@
         for n, (source, ref) in enumerate(zip(sources, held))
     ]
     rows.start()
-    for copy in copies:
+    for copy in copies[:4]:
         copy.start()
     x_ref, ga_ref, ua_ref, gb_ref, ub_ref, da_ref, db_ref = held
     rows.wait()
+    for copy in copies[4:]:
+        copy.start()
     unpack(x_ref, dense_ref)
     x = dense_ref[...]
     copies[0].wait()
@@ -288,17 +332,17 @@
 
 
 def combine_kernel(base, own_ref, values_ref, routes_ref, weight_ref, *refs):
-    del own_ref
-    copy = None
-    if base:
-        source, out_ref, before_ref, sem = refs
-        copy = pltpu.make_async_copy(source, before_ref, sem)
-        copy.start()
+    first = bool(base == 0)
+    if first:
+        (out_ref,) = refs
     else:
-        (out_ref,) = refs
+        source, out_hbm, before_ref, out_ref, sem, out_sems = refs
+        fetch = pltpu.make_async_copy(source, before_ref, sem)
+        fetch.start()
     rows, tokens = values_ref.shape[0], out_ref.shape[0]
-    routes = jnp.transpose(routes_ref[...].astype(F32)).astype(jnp.int32)
-    weights = jnp.transpose(weight_ref[...])
+    lanes = pl.ds(pl.multiple_of(own_ref[0] * tokens, tokens), tokens)
+    routes = jnp.transpose(routes_ref[:, lanes].astype(F32)).astype(jnp.int32)
+    weights = jnp.transpose(weight_ref[:, lanes])
     row = lax.broadcasted_iota(jnp.int32, (tokens, rows), 1)
     expert, sub = row // SUB, row % SUB
     by_first, by_second = expert == routes[:, 0:1], expert == routes[:, 1:2]
@@ -316,7 +360,20 @@
     def split(chosen):
         return [jnp.where(chosen, part, 0.0).astype(BF16) for part in (high, low)]
 
-    totals = {}
+    copies = []
+
+    def put(total, start):
+        columns = slice(start, start + PIECE)
+        if first:
+            out_ref[:, columns] = total
+            return
+        if not copies:
+            fetch.wait()
+        out_ref[:, columns] = (total + before_ref[:, columns]).astype(BF16)
+        copies.append(column_copy(out_ref, out_hbm, start, PIECE, out_sems.at[len(copies)]))
+        copies[-1].start()
+
+    tails = {}
     mains = [part for h in range(2) for part in split(main_place(sub, slot, h))]
     for c in range(FOLD):
         maps = list(mains)
@@ -325,38 +382,42 @@
                 maps += split(tail_place(sub, slot, u, c))
         found = dot(jnp.concatenate(maps, axis=0), values_ref[:, c * PIECE : (c + 1) * PIECE])
         for n, start in enumerate(dense_columns(c)):
-            block = found[2 * n * tokens : (2 * n + 1) * tokens] + found[(2 * n + 1) * tokens : (2 * n + 2) * tokens]
-            totals[start] = totals[start] + block if start in totals else block
-    if copy is not None:
+            at = 2 * n * tokens
+            block = found[at : at + tokens] + found[at + tokens : at + 2 * tokens]
+            if start < MAIN:
+                put(block, start)
+            else:
+                tails[start] = tails[start] + block if start in tails else block
+    for start, total in tails.items():
+        put(total, start)
+    for copy in copies:
         copy.wait()
-    for start, total in totals.items():
-        columns = slice(start, start + PIECE)
-        if copy is not None:
-            total += before_ref[:, columns]
-        out_ref[:, columns] = total.astype(out_ref.dtype)
 
 
 def combine(chunk, values, routes_t, weight_t, own, tokens, before=None):
-    rest = () if before is None else (before,)
+    first = before is None
+    pieces = WIDTH // PIECE
     return pl.pallas_call(
         partial(combine_kernel, chunk * SLOTS),
-        out_shape=jax.ShapeDtypeStruct((tokens, WIDTH), F32 if before is None else BF16),
+        out_shape=jax.ShapeDtypeStruct((tokens, WIDTH), F32 if first else BF16),
         grid_spec=pltpu.PrefetchScalarGridSpec(
             num_scalar_prefetch=1,
             grid=(1,),
-            in_specs=[
-                VMEM,
-                pl.BlockSpec((K, tokens), lambda i, own: (0, own[0])),
-                pl.BlockSpec((K, tokens), lambda i, own: (0, own[0])),
-            ]
-            + [ANY] * len(rest),
-            out_specs=VMEM if before is None else pl.BlockSpec((tokens, WIDTH), lambda i, own: (0, 0)),
-            scratch_shapes=[pltpu.VMEM((tokens, WIDTH), F32), pltpu.SemaphoreType.DMA] if rest else [],
+            in_specs=[VMEM] * 3 + ([] if first else [ANY]),
+            out_specs=VMEM if first else ANY,
+            scratch_shapes=[]
+            if first
+            else [
+                pltpu.VMEM((tokens, WIDTH), F32),
+                pltpu.VMEM((tokens, WIDTH), BF16),
+                pltpu.SemaphoreType.DMA,
+                pltpu.SemaphoreType.DMA((pieces,)),
+            ],
         ),
         cost_estimate=pl.CostEstimate(flops=1_500_000_000, bytes_accessed=2_100_000, transcendentals=0),
         compiler_params=pltpu.CompilerParams(vmem_limit_bytes=LARGE),
         name="combine",
-    )(own, values, routes_t, weight_t, *rest)
+    )(own, values, routes_t, weight_t, *(() if first else (before,)))
 
 
 def exchanged(rows):
@@ -407,9 +468,7 @@
         expert_out = combine(n, returned, routes_t, weight_t, own, tokens, expert_out)
 
     extended = jnp.concatenate([before, pool_in], axis=0).astype(F32)
-    positions = (
-        lax.axis_index(("ep", "tp")) * rows_here + jnp.arange(rows_here)
-    ).astype(F32)
+    positions = (lax.axis_index(("ep", "tp")) * rows_here + jnp.arange(rows_here)).astype(F32)
     pooled = pooled_rows(extended, positions)
     group_count = w_pool.shape[0]
     grouped = jnp.einsum(

time: 157 us -> 156 us (level)
  Pallas kernels: 30.2 us -> 28.6 us
where the time goes in v2:
time: 156 us; the launch traced here: 155 us
  waiting for transfers between devices  64.3 us (41%)
  starting transfers between devices  56.8 us (36%)
  Pallas kernels  28.6 us (18%)
  matrix products  4.18 us (3%)
    all_to_all x4, starting transfers between devices, exchanged(): lax.all_to_all(rows.reshape(experts, SUB, LANES), 'ep', split_axis=0, con...  45.1 us
    all_to_all x4, waiting for transfers between devices, exchanged(): lax.all_to_all(rows.reshape(experts, SUB, LANES), 'ep', split_axis=0, con...  37.1 us
    ppermute x7, waiting for transfers between devices, swapped(): return lax.ppermute(array, ('ep', 'tp'), pairs)  26.2 us
    pallas_call x4, Pallas kernels, half_ffn(): pl.pallas_call(ffn_kernel, out_shape=jax.ShapeDtypeStruct((dense, WIDTH),...  14 us
    ppermute x7, starting transfers between devices, swapped(): return lax.ppermute(array, ('ep', 'tp'), pairs)  9.75 us
    pallas_call x2, Pallas kernels, send_rows(): pl.pallas_call(partial(send_kernel, chunk * SLOTS), out_shape=jax.ShapeDt...  5.49 us
    pallas_call x2, Pallas kernels, combine(): pl.pallas_call(partial(combine_kernel, chunk * SLOTS), out_shape=jax.Shap...  4.65 us
    pallas_call x2, Pallas kernels, pack_sum(): pl.pallas_call(pack_kernel, out_shape=jax.ShapeDtypeStruct((rows, LANES),...  4.41 us
  transfers between devices with their start and end apart: 12, of which 9 were waited for; matrix products, arithmetic and copies ran while one was open for 3% of the time, Pallas kernels for 15%

profile of v2, /device:TPU:1, one launch (start us, length us, event | category | flops | bytes accessed | tf_op | source)
XLA Modules:
  0.0 155.4 jit_solution(13617575877859793356)
XLA Ops:
  0.6 2.8 %send_rows.3 = bf16[512,768]{1,0:T(8,128)(2,1)} custom-call(s32[1]{0:T(128)} %bitcast.2.own_ref, bf16[512,2048]{1,0:T(8,128)(2,1)} %rows_hbm.3, f32[1,2048]{1,0:T(1,128)} %bitcast.45, s32[2,512]{1,0:T(2,128)} %bitcast.37), custom_call_target="tpu_custom_call" | custom-call | flops 2000000000 | bytes 2100000 | tf_op jit(solution)/shard_map/send_rows/pallas_call | solution.py:170
  3.4 13.0 %all-to-all-start.2 = ((bf16[64,8,768]{2,1,0:T(8,128)(2,1)}), bf16[64,8,768]{2,1,0:T(8,128)(2,1)S(1)}, u32[]{:S(2)}, u32[]{:S(2)}) async-start(bf16[64,8,768]{2,1,0:T(8,128)(2,1)} %bitcast.44), calls=%async_computation.2 | async-start | bytes 1572864 | tf_op jit(solution)/shard_map/all_to_all | solution.py:425
  16.4 2.8 %collective-permute-start.1 = (bf16[2048,256]{1,0:T(8,128)(2,1)}, bf16[2048,256]{1,0:T(8,128)(2,1)}, u32[]{:S(2)}, u32[]{:S(2)}) collective-permute-start(bf16[2048,256]{1,0:T(8,128)(2,1)} %bitcast.7.refs_1_), channel_id=1, source_target_pairs={{0,1},{1,0},{2,3},{3,2},{4,7},{5,6},{6,5},{7,4},{8,9},{9,8},{10,11... | collective-permute-start | bytes 3145736 | tf_op jit(solution)/shard_map/ppermute | solution.py:48
  19.4 2.6 %collective-permute-start.3 = (bf16[256,2048]{1,0:T(8,128)(2,1)}, bf16[256,2048]{1,0:T(8,128)(2,1)}, u32[]{:S(2)}, u32[]{:S(2)}) collective-permute-start(bf16[256,2048]{1,0:T(8,128)(2,1)} %bitcast.9.refs_5_), channel_id=1, source_target_pairs={{0,1},{1,0},{2,3},{3,2},{4,7},{5,6},{6,5},{7,4},{8,9},{9,8},{10,11... | collective-permute-start | bytes 3145736 | tf_op jit(solution)/shard_map/ppermute | solution.py:48
  21.9 2.7 %send_rows.2 = bf16[512,768]{1,0:T(8,128)(2,1)} custom-call(s32[1]{0:T(128)} %bitcast.2.own_ref, bf16[512,2048]{1,0:T(8,128)(2,1)} %rows_hbm.3, f32[1,2048]{1,0:T(1,128)} %bitcast.46, s32[2,512]{1,0:T(2,128)} %bitcast.38), custom_call_target="tpu_custom_call" | custom-call | flops 2000000000 | bytes 2100000 | tf_op jit(solution)/shard_map/send_rows/pallas_call | solution.py:170
  24.6 14.8 %all-to-all-done.2 = bf16[64,8,768]{2,1,0:T(8,128)(2,1)S(1)} async-done(((bf16[64,8,768]{2,1,0:T(8,128)(2,1)}), bf16[64,8,768]{2,1,0:T(8,128)(2,1)S(1)}, u32[]{:S(2)}, u32[]{:S(2)}) %all-to-all-start.2) | async-done | bytes 786464 | tf_op jit(solution)/shard_map/all_to_all | solution.py:425
  39.4 5.9 %all-to-all-start = ((bf16[64,8,768]{2,1,0:T(8,128)(2,1)}), bf16[64,8,768]{2,1,0:T(8,128)(2,1)S(1)}, u32[]{:S(2)}, u32[]{:S(2)}) async-start(bf16[64,8,768]{2,1,0:T(8,128)(2,1)} %bitcast.43), calls=%async_computation | async-start | bytes 1572864 | tf_op jit(solution)/shard_map/all_to_all | solution.py:425
  46.7 11.8 %collective-permute-done.3.refs_6_ = bf16[256,2048]{1,0:T(8,128)(2,1)} collective-permute-done((bf16[256,2048]{1,0:T(8,128)(2,1)}, bf16[256,2048]{1,0:T(8,128)(2,1)}, u32[]{:S(2)}, u32[]{:S(2)}) %collective-permute-start.3) | collective-permute-done | bytes 1048608 | tf_op jit(solution)/shard_map/ppermute | solution.py:48
  58.6 3.9 %collective-permute-done.6.refs_0_ = bf16[512,768]{1,0:T(8,128)(2,1)S(1)} collective-permute-done((bf16[512,768]{1,0:T(8,128)(2,1)S(1)}, bf16[512,768]{1,0:T(8,128)(2,1)S(1)}, u32[]{:S(2)}, u32[]{:S(2)}) %collective-permute-start.6) | collective-permute-done | bytes 786464 | tf_op jit(solution)/shard_map/ppermute | solution.py:48
  62.5 3.5 %half_ffn.7 = bf16[192,2048]{1,0:T(8,128)(2,1)S(1)} custom-call(bf16[512,768]{1,0:T(8,128)(2,1)S(1)} %collective-permute-done.6.refs_0_, bf16[2048,256]{1,0:T(8,128)(2,1)} %bitcast.7.refs_1_, bf16[2048,256]{1,0:T(8,128)(2,1)} %bitcast.8.refs_2_, bf16[2048,256]{1,0:T(8,128)(2,1)} %collective-permute-done.1.refs_3_, ...), custom_call_target="tpu_custom_call" | custom-call | flops 3500000000 | bytes 7864320 | tf_op jit(solution)/shard_map/half_ffn/pallas_call | solution.py:316
  69.6 3.5 %half_ffn.6.a_ref = bf16[192,2048]{1,0:T(8,128)(2,1)S(1)} custom-call(bf16[512,768]{1,0:T(8,128)(2,1)S(1)} %bitcast.35, bf16[2048,256]{1,0:T(8,128)(2,1)} %bitcast.7.refs_1_, bf16[2048,256]{1,0:T(8,128)(2,1)} %bitcast.8.refs_2_, bf16[2048,256]{1,0:T(8,128)(2,1)} %collective-permute-done.1.refs_3_, bf16[2048,256]{1,0:T(8,128)(2,1)} %collective-permute-done.2.refs_4_, ...), custom_call_target="tpu_custom_call" | custom-call | flops 3500000000 | bytes 7864320 | tf_op jit(solution)/shard_map/half_ffn/pallas_call | solution.py:316
  73.2 4.2 %collective-permute-done.7.b_ref = bf16[192,2048]{1,0:T(8,128)(2,1)} collective-permute-done((bf16[192,2048]{1,0:T(8,128)(2,1)S(1)}, bf16[192,2048]{1,0:T(8,128)(2,1)}, u32[]{:S(2)}, u32[]{:S(2)}) %collective-permute-start.7) | collective-permute-done | bytes 786464 | tf_op jit(solution)/shard_map/ppermute | solution.py:48
  77.3 2.7 %pack_sum.3 = bf16[512,768]{1,0:T(8,128)(2,1)} custom-call(bf16[192,2048]{1,0:T(8,128)(2,1)S(1)} %half_ffn.6.a_ref, bf16[192,2048]{1,0:T(8,128)(2,1)} %collective-permute-done.7.b_ref), custom_call_target="tpu_custom_call" | custom-call | flops 800000000 | bytes 2359296 | tf_op jit(solution)/shard_map/pack_sum/pallas_call | solution.py:269
  80.1 12.9 %all-to-all-start.3 = ((bf16[64,8,768]{2,1,0:T(8,128)(2,1)}), bf16[64,8,768]{2,1,0:T(8,128)(2,1)S(1)}, u32[]{:S(2)}, u32[]{:S(2)}) async-start(bf16[64,8,768]{2,1,0:T(8,128)(2,1)} %bitcast.15), calls=%async_computation.3 | async-start | bytes 1572864 | tf_op jit(solution)/shard_map/all_to_all | solution.py:425
  93.0 1.9 %collective-permute-start = (bf16[15,1024]{1,0:T(8,128)(2,1)S(1)}, bf16[15,1024]{1,0:T(8,128)(2,1)S(1)}, u32[]{:S(2)}, u32[]{:S(2)}) collective-permute-start(bf16[15,1024]{1,0:T(8,128)(2,1)S(1)} %slice.52), channel_id=1, source_target_pairs={{0,1},{1,2},{2,3},{3,4},{4,5},{5,6},{6,7},{7,8},{8,9},{9,10},{10,1... | collective-permute-start | bytes 92168 | tf_op jit(solution)/shard_map/ppermute | solution.py:38
  95.0 3.5 %half_ffn.5 = bf16[192,2048]{1,0:T(8,128)(2,1)S(1)} custom-call(bf16[512,768]{1,0:T(8,128)(2,1)S(1)} %collective-permute-done.4.refs_0_, bf16[2048,256]{1,0:T(8,128)(2,1)} %bitcast.7.refs_1_, bf16[2048,256]{1,0:T(8,128)(2,1)} %bitcast.8.refs_2_, bf16[2048,256]{1,0:T(8,128)(2,1)} %collective-permute-done.1.refs_3_, ...), custom_call_target="tpu_custom_call" | custom-call | flops 3500000000 | bytes 7864320 | tf_op jit(solution)/shard_map/half_ffn/pallas_call | solution.py:316
  100.0 3.5 %half_ffn.4.a_ref = bf16[192,2048]{1,0:T(8,128)(2,1)S(1)} custom-call(bf16[512,768]{1,0:T(8,128)(2,1)S(1)} %bitcast.32, bf16[2048,256]{1,0:T(8,128)(2,1)} %bitcast.7.refs_1_, bf16[2048,256]{1,0:T(8,128)(2,1)} %bitcast.8.refs_2_, bf16[2048,256]{1,0:T(8,128)(2,1)} %collective-permute-done.1.refs_3_, bf16[2048,256]{1,0:T(8,128)(2,1)} %collective-permute-done.2.refs_4_, ...), custom_call_target="tpu_custom_call" | custom-call | flops 3500000000 | bytes 7864320 | tf_op jit(solution)/shard_map/half_ffn/pallas_call | solution.py:316
  103.5 6.2 %collective-permute-done.5.b_ref = bf16[192,2048]{1,0:T(8,128)(2,1)S(1)} collective-permute-done((bf16[192,2048]{1,0:T(8,128)(2,1)S(1)}, bf16[192,2048]{1,0:T(8,128)(2,1)S(1)}, u32[]{:S(2)}, u32[]{:S(2)}) %collective-permute-start.5) | collective-permute-done | bytes 786464 | tf_op jit(solution)/shard_map/ppermute | solution.py:48
  111.4 4.6 %all-to-all-done.3 = bf16[64,8,768]{2,1,0:T(8,128)(2,1)S(1)} async-done(((bf16[64,8,768]{2,1,0:T(8,128)(2,1)}), bf16[64,8,768]{2,1,0:T(8,128)(2,1)S(1)}, u32[]{:S(2)}, u32[]{:S(2)}) %all-to-all-start.3) | async-done | bytes 786464 | tf_op jit(solution)/shard_map/all_to_all | solution.py:425
  116.0 13.4 %all-to-all-start.1 = ((bf16[64,8,768]{2,1,0:T(8,128)(2,1)}), bf16[64,8,768]{2,1,0:T(8,128)(2,1)S(1)}, u32[]{:S(2)}, u32[]{:S(2)}) async-start(bf16[64,8,768]{2,1,0:T(8,128)(2,1)} %bitcast.10), calls=%async_computation.1 | async-start | bytes 1572864 | tf_op jit(solution)/shard_map/all_to_all | solution.py:425
  129.4 1.9 %fusion.5 = f32[8,256,128]{1,2,0:T(8,128)S(1)} fusion(bf16[8,128,128]{2,1,0:T(8,128)(2,1)S(1)} %copy-done, f32[1024]{0:T(1024)S(1)} %select_select_fusion, f32[256]{0:T(256)S(1)} %convert_add_fusion, pred[1024]{0:T(1024)(128)(4,1)S(1)} %get-tuple-element.5, pred[1024]{0:T(1024)(128)(4,1)S(1)} %get-tuple-element.4, ...), kind=kOutput, calls=%fused_computation.23 | convolution fusion | flops 73138176 | bytes 18097152 | tf_op jit(solution)/shard_map/tgc,gcd->tgd/dot_general | solution.py:474
  131.6 2.2 %convolution_convert_fusion = bf16[256,2048]{1,0:T(8,128)(2,1)} fusion(bf16[256,1024]{0,1:T(8,128)(2,1)S(1)} %fusion.3, bf16[1024,2048]{1,0:T(8,128)(2,1)S(1)} %copy-done.5), kind=kOutput, calls=%fused_computation | convolution fusion | flops 1074266112 | bytes 5767168 | tf_op jit(solution)/shard_map/dot_general | solution.py:77
  135.6 16.7 %all-to-all-done.1 = bf16[64,8,768]{2,1,0:T(8,128)(2,1)S(1)} async-done(((bf16[64,8,768]{2,1,0:T(8,128)(2,1)}), bf16[64,8,768]{2,1,0:T(8,128)(2,1)S(1)}, u32[]{:S(2)}, u32[]{:S(2)}) %all-to-all-start.1) | async-done | bytes 786464 | tf_op jit(solution)/shard_map/all_to_all | solution.py:425
  152.4 2.9 %combine.3 = bf16[128,2048]{1,0:T(8,128)(2,1)} custom-call(s32[1]{0:T(128)} %bitcast.2.own_ref, bf16[512,768]{1,0:T(8,128)(2,1)S(1)} %bitcast.36, s32[2,512]{1,0:T(2,128)S(1)} %bitcast.40, f32[2,512]{1,0:T(2,128)S(1)} %bitcast.42, f32[128,2048]{1,0:T(8,128)S(1)} %combine.2.refs_0_), custom_call_target="tpu_custom_call" | custom-call | flops 1500000000 | bytes 2100000 | tf_op jit(solution)/shard_map/combine/pallas_call | solution.py:400
  (31 shorter events, 10.3 us)
Async XLA Ops:
  0.6 128.7 %copy-start = (bf16[8,128,128]{2,1,0:T(8,128)(2,1)S(1)}, bf16[8,128,128]{2,1,0:T(8,128)(2,1)}, u32[]{:S(2)}) copy-start(bf16[8,128,128]{2,1,0:T(8,128)(2,1)} %param.12) | copy-start | bytes 786436
  3.4 36.0 %all-to-all-start.2 = ((bf16[64,8,768]{2,1,0:T(8,128)(2,1)}), bf16[64,8,768]{2,1,0:T(8,128)(2,1)S(1)}, u32[]{:S(2)}, u32[]{:S(2)}) async-start(bf16[64,8,768]{2,1,0:T(8,128)(2,1)} %bitcast.44), calls=%async_computation.2 | async-start | bytes 1572864 | tf_op jit(solution)/shard_map/all_to_all | solution.py:425
  16.4 30.3 %collective-permute-start.1 = (bf16[2048,256]{1,0:T(8,128)(2,1)}, bf16[2048,256]{1,0:T(8,128)(2,1)}, u32[]{:S(2)}, u32[]{:S(2)}) collective-permute-start(bf16[2048,256]{1,0:T(8,128)(2,1)} %bitcast.7.refs_1_), channel_id=1, source_target_pairs={{0,1},{1,0},{2,3},{3,2},{4,7},{5,6},{6,5},{7,4},{8,9},{9,8},{10,11... | collective-permute-start | bytes 3145736 | tf_op jit(solution)/shard_map/ppermute | solution.py:48
  19.3 27.5 %collective-permute-start.2 = (bf16[2048,256]{1,0:T(8,128)(2,1)}, bf16[2048,256]{1,0:T(8,128)(2,1)}, u32[]{:S(2)}, u32[]{:S(2)}) collective-permute-start(bf16[2048,256]{1,0:T(8,128)(2,1)} %bitcast.8.refs_2_), channel_id=1, source_target_pairs={{0,1},{1,0},{2,3},{3,2},{4,7},{5,6},{6,5},{7,4},{8,9},{9,8},{10,11... | collective-permute-start | bytes 3145736 | tf_op jit(solution)/shard_map/ppermute | solution.py:48
  19.4 39.2 %collective-permute-start.3 = (bf16[256,2048]{1,0:T(8,128)(2,1)}, bf16[256,2048]{1,0:T(8,128)(2,1)}, u32[]{:S(2)}, u32[]{:S(2)}) collective-permute-start(bf16[256,2048]{1,0:T(8,128)(2,1)} %bitcast.9.refs_5_), channel_id=1, source_target_pairs={{0,1},{1,0},{2,3},{3,2},{4,7},{5,6},{6,5},{7,4},{8,9},{9,8},{10,11... | collective-permute-start | bytes 3145736 | tf_op jit(solution)/shard_map/ppermute | solution.py:48
  39.4 28.9 %all-to-all-start = ((bf16[64,8,768]{2,1,0:T(8,128)(2,1)}), bf16[64,8,768]{2,1,0:T(8,128)(2,1)S(1)}, u32[]{:S(2)}, u32[]{:S(2)}) async-start(bf16[64,8,768]{2,1,0:T(8,128)(2,1)} %bitcast.43), calls=%async_computation | async-start | bytes 1572864 | tf_op jit(solution)/shard_map/all_to_all | solution.py:425
  45.3 17.1 %collective-permute-start.6 = (bf16[512,768]{1,0:T(8,128)(2,1)S(1)}, bf16[512,768]{1,0:T(8,128)(2,1)S(1)}, u32[]{:S(2)}, u32[]{:S(2)}) collective-permute-start(bf16[512,768]{1,0:T(8,128)(2,1)S(1)} %bitcast.34), channel_id=1, source_target_pairs={{0,3},{1,2},{2,1},{3,0},{4,5},{5,4},{6,7},{7,6},{8,11},{9,10},{10,... | collective-permute-start | bytes 2359304 | tf_op jit(solution)/shard_map/ppermute | solution.py:48
  66.0 11.3 %collective-permute-start.7 = (bf16[192,2048]{1,0:T(8,128)(2,1)S(1)}, bf16[192,2048]{1,0:T(8,128)(2,1)}, u32[]{:S(2)}, u32[]{:S(2)}) collective-permute-start(bf16[192,2048]{1,0:T(8,128)(2,1)S(1)} %half_ffn.7), channel_id=1, source_target_pairs={{0,3},{1,2},{2,1},{3,0},{4,5},{5,4},{6,7},{7,6},{8,11},{9,10},{10,... | collective-permute-start | bytes 2359304 | tf_op jit(solution)/shard_map/ppermute | solution.py:48
  68.3 26.6 %collective-permute-start.4 = (bf16[512,768]{1,0:T(8,128)(2,1)S(1)}, bf16[512,768]{1,0:T(8,128)(2,1)S(1)}, u32[]{:S(2)}, u32[]{:S(2)}) collective-permute-start(bf16[512,768]{1,0:T(8,128)(2,1)S(1)} %bitcast.31), channel_id=1, source_target_pairs={{0,3},{1,2},{2,1},{3,0},{4,5},{5,4},{6,7},{7,6},{8,11},{9,10},{10,... | collective-permute-start | bytes 2359304 | tf_op jit(solution)/shard_map/ppermute | solution.py:48
  80.1 12.9 %copy-start.3 = (bf16[256,1024]{1,0:T(8,128)(2,1)S(1)}, bf16[256,1024]{1,0:T(8,128)(2,1)}, u32[]{:S(2)}) copy-start(bf16[256,1024]{1,0:T(8,128)(2,1)} %param.11) | copy-start | bytes 1572868
  80.1 35.9 %all-to-all-start.3 = ((bf16[64,8,768]{2,1,0:T(8,128)(2,1)}), bf16[64,8,768]{2,1,0:T(8,128)(2,1)S(1)}, u32[]{:S(2)}, u32[]{:S(2)}) async-start(bf16[64,8,768]{2,1,0:T(8,128)(2,1)} %bitcast.15), calls=%async_computation.3 | async-start | bytes 1572864 | tf_op jit(solution)/shard_map/all_to_all | solution.py:425
  93.0 6.8 %collective-permute-start = (bf16[15,1024]{1,0:T(8,128)(2,1)S(1)}, bf16[15,1024]{1,0:T(8,128)(2,1)S(1)}, u32[]{:S(2)}, u32[]{:S(2)}) collective-permute-start(bf16[15,1024]{1,0:T(8,128)(2,1)S(1)} %slice.52), channel_id=1, source_target_pairs={{0,1},{1,2},{2,3},{3,4},{4,5},{5,6},{6,7},{7,8},{8,9},{9,10},{10,1... | collective-permute-start | bytes 92168 | tf_op jit(solution)/shard_map/ppermute | solution.py:38
  98.5 11.2 %collective-permute-start.5 = (bf16[192,2048]{1,0:T(8,128)(2,1)S(1)}, bf16[192,2048]{1,0:T(8,128)(2,1)S(1)}, u32[]{:S(2)}, u32[]{:S(2)}) collective-permute-start(bf16[192,2048]{1,0:T(8,128)(2,1)S(1)} %half_ffn.5), channel_id=1, source_target_pairs={{0,3},{1,2},{2,1},{3,0},{4,5},{5,4},{6,7},{7,6},{8,11},{9,10},{10,... | collective-permute-start | bytes 2359304 | tf_op jit(solution)/shard_map/ppermute | solution.py:48
  116.0 36.4 %all-to-all-start.1 = ((bf16[64,8,768]{2,1,0:T(8,128)(2,1)}), bf16[64,8,768]{2,1,0:T(8,128)(2,1)S(1)}, u32[]{:S(2)}, u32[]{:S(2)}) async-start(bf16[64,8,768]{2,1,0:T(8,128)(2,1)} %bitcast.10), calls=%async_computation.1 | async-start | bytes 1572864 | tf_op jit(solution)/shard_map/all_to_all | solution.py:425
  129.4 2.0 %copy-start.4 = (f32[1024]{0:T(1024)S(1)}, f32[1024]{0:T(1024)}, u32[]{:S(2)}) copy-start(f32[1024]{0:T(1024)} %param.13) | copy-start | bytes 12292
  129.4 2.2 %copy-start.5 = (bf16[1024,2048]{1,0:T(8,128)(2,1)S(1)}, bf16[1024,2048]{1,0:T(8,128)(2,1)}, u32[]{:S(2)}) copy-start(bf16[1024,2048]{1,0:T(8,128)(2,1)} %param.14) | copy-start | bytes 12582916
  131.6 2.3 %copy-start.1 = (s32[512,2]{0,1:T(2,128)S(1)}, s32[512,2]{0,1:T(2,128)}, u32[]{:S(2)}) copy-start(s32[512,2]{0,1:T(2,128)} %param.17) | copy-start | bytes 12292
  131.6 2.3 %copy-start.2 = (f32[512,2]{0,1:T(2,128)S(1)}, f32[512,2]{0,1:T(2,128)}, u32[]{:S(2)}) copy-start(f32[512,2]{0,1:T(2,128)} %param.18) | copy-start | bytes 12292

commit v3 on v1

--- a/solution.py
+++ b/solution.py
@@ -102,26 +102,49 @@
     return any((r * FOLD + c - piece) % 2 == 0 for r in range(SUB - 2 * SLOTS))
 
 
-def send_kernel(base, own_ref, rows_hbm, gain_ref, routes_ref, out_ref, rows_ref, normed_ref, sems):
+def send_kernel(
+    base,
+    own_ref,
+    rows_hbm,
+    gain_hbm,
+    routes_hbm,
+    out_hbm,
+    rows_ref,
+    normed_ref,
+    gain_ref,
+    routes_ref,
+    out_ref,
+    sems,
+    out_sems,
+):
     tokens = rows_ref.shape[0]
     half = tokens // 2
-    copies = []
-    for n in range(2):
-        here = pl.ds(pl.multiple_of(own_ref[0] * tokens + n * half, half), half)
-        copies.append(
-            pltpu.make_async_copy(
-                rows_hbm.at[here], rows_ref.at[pl.ds(n * half, half)], sems.at[n]
-            )
+    first = pl.multiple_of(own_ref[0] * tokens, tokens)
+    fetches = [
+        pltpu.make_async_copy(routes_hbm.at[:, pl.ds(first, tokens)], routes_ref, sems.at[2]),
+        pltpu.make_async_copy(gain_hbm, gain_ref, sems.at[3]),
+    ]
+    halves = [
+        pltpu.make_async_copy(
+            rows_hbm.at[pl.ds(pl.multiple_of(first + n * half, half), half)],
+            rows_ref.at[pl.ds(n * half, half)],
+            sems.at[n],
         )
-        copies[n].start()
+        for n in range(2)
+    ]
+    for copy in fetches + halves:
+        copy.start()
+    fetches[0].wait()
     _, named, rank, sub = slot_ranks(routes_ref, out_ref.shape[0], tokens, base)
     mains = jnp.concatenate([as_bf16(named & main_place(sub, rank, h)) for h in range(2)], axis=1)
+    fetches[1].wait()
     for n in range(2):
         here = slice(n * half, (n + 1) * half)
-        copies[n].wait()
+        halves[n].wait()
         features = rows_ref[here, :].astype(F32)
         inverse = lax.rsqrt(jnp.mean(features * features, axis=-1, keepdims=True) + EPS)
         normed_ref[here, :] = (features * inverse * gain_ref[...]).astype(BF16)
+    outs = []
     for c in range(FOLD):
         used = [u for u in range(2) if tail_used(u, c)]
         tails = [as_bf16(named & tail_place(sub, rank, u, c)) for u in used]
@@ -130,6 +153,15 @@
             jnp.concatenate([mains, *tails], axis=1),
             jnp.concatenate([normed_ref[:, start : start + PIECE] for start in starts], axis=0),
         ).astype(BF16)
+        outs.append(column_copy(out_ref, out_hbm, c * PIECE, PIECE, out_sems.at[c]))
+        outs[-1].start()
+    for copy in outs:
+        copy.wait()
+
+
+def column_copy(source, target, at, width, sem):
+    columns = pl.ds(at, width)
+    return pltpu.make_async_copy(source.at[:, columns], target.at[:, columns], sem)
 
 
 def send_rows(expert_in, gain, routes_t, own, experts, chunk):
@@ -141,13 +173,17 @@
         grid_spec=pltpu.PrefetchScalarGridSpec(
             num_scalar_prefetch=1,
             grid=(1,),
-            in_specs=[
-                ANY,
-                pl.BlockSpec((1, width), lambda i, own: (0, 0)),
-                pl.BlockSpec((K, tokens), lambda i, own: (0, own[0])),
+            in_specs=[ANY] * 3,
+            out_specs=ANY,
+            scratch_shapes=[
+                pltpu.VMEM((tokens, width), BF16),
+                pltpu.VMEM((tokens, width), BF16),
+                pltpu.VMEM((1, width), F32),
+                pltpu.VMEM((K, tokens), jnp.int32),
+                pltpu.VMEM((experts * SUB, LANES), BF16),
+                pltpu.SemaphoreType.DMA((4,)),
+                pltpu.SemaphoreType.DMA((FOLD,)),
             ],
-            out_specs=VMEM,
-            scratch_shapes=[pltpu.VMEM((tokens, width), BF16)] * 2 + [pltpu.SemaphoreType.DMA((2,))],
         ),
         cost_estimate=pl.CostEstimate(flops=2_000_000_000, bytes_accessed=2_100_000, transcendentals=128),
         name="send_rows",
@@ -203,7 +239,8 @@
         put(block, g, start)
 
 
-def pack_kernel(a_ref, b_ref, out_ref):
+def pack_kernel(a_ref, b_ref, out_hbm, out_ref, sems):
+    copies = []
     experts = out_ref.shape[0] // SUB
     mains = main_maps((GROUP, DENSE), 1)
     for c in range(FOLD):
@@ -221,6 +258,10 @@
             out_ref[g * GROUP : (g + 1) * GROUP, c * PIECE : (c + 1) * PIECE] = dot(
                 maps, jnp.concatenate(pieces, axis=0)
             ).astype(BF16)
+        copies.append(column_copy(out_ref, out_hbm, c * PIECE, PIECE, sems.at[c]))
+        copies[-1].start()
+    for copy in copies:
+        copy.wait()
 
 
 def pack_sum(a, b):
@@ -229,7 +270,8 @@
         pack_kernel,
         out_shape=jax.ShapeDtypeStruct((rows, LANES), BF16),
         in_specs=[VMEM] * 2,
-        out_specs=VMEM,
+        out_specs=ANY,
+        scratch_shapes=[pltpu.VMEM((rows, LANES), BF16), pltpu.SemaphoreType.DMA((FOLD,))],
         cost_estimate=pl.CostEstimate(flops=800_000_000, bytes_accessed=a.size * 6, transcendentals=0),
         compiler_params=pltpu.CompilerParams(vmem_limit_bytes=SMALL),
         name="pack_sum",
@@ -243,14 +285,18 @@
         for n, (source, ref) in enumerate(zip(sources, held))
     ]
     rows.start()
-    for copy in copies:
+    for copy in copies[:2]:
         copy.start()
     x_ref, ga_ref, ua_ref, gb_ref, ub_ref, da_ref, db_ref = held
     rows.wait()
+    for copy in copies[2:4]:
+        copy.start()
     unpack(x_ref, dense_ref)
     x = dense_ref[...]
     copies[0].wait()
     copies[1].wait()
+    for copy in copies[4:]:
+        copy.start()
     hidden_a = (jax.nn.silu(dot(x, ga_ref[...])) * dot(x, ua_ref[...])).astype(BF16)
     copies[2].wait()
     copies[3].wait()
@@ -388,7 +434,8 @@
     before = passed_along(pool_in[rows_here - (WMAX - 1) :], ("ep", "tp"), 1)
 
     gate, up, down = w_gate[0], w_up[0], w_down[0]
-    gate_b, up_b = swapped(gate, 0), swapped(up, 0)
+    gate_b = swapped(gate, 0)
+    up_b = swapped(up, 0)
     down_b = swapped(down, 0)
     ffn = lambda x: half_ffn(x, gate, gate_b, up, up_b, down, down_b)
 

time: 157 us -> 157 us (level)
    pallas_call x4, Pallas kernels: 14 us -> 15.8 us  [half_ffn(): pl.pallas_call(ffn_kernel, out_shape=jax.ShapeDtypeStruct((dense, WIDTH),...]
  transfers between devices with their start and end apart: 12 -> 12, of which waited for: 9 -> 9; matrix products, arithmetic and copies ran while one was open for 3% -> 3% of each run, Pallas kernels for 15% -> 16%
where the time goes in v3:
time: 157 us; the launch traced here: 156 us
  waiting for transfers between devices  63.1 us (40%)
  starting transfers between devices  57.4 us (37%)
  Pallas kernels  30.2 us (19%)
  matrix products  4.18 us (3%)
    all_to_all x4, starting transfers between devices, exchanged(): lax.all_to_all(rows.reshape(experts, SUB, LANES), 'ep', split_axis=0, con...  45.7 us
    all_to_all x4, waiting for transfers between devices, exchanged(): lax.all_to_all(rows.reshape(experts, SUB, LANES), 'ep', split_axis=0, con...  36.2 us
    ppermute x7, waiting for transfers between devices, swapped(): return lax.ppermute(array, ('ep', 'tp'), pairs)  26.2 us
    pallas_call x4, Pallas kernels, half_ffn(): pl.pallas_call(ffn_kernel, out_shape=jax.ShapeDtypeStruct((dense, WIDTH),...  15.8 us
    ppermute x7, starting transfers between devices, swapped(): return lax.ppermute(array, ('ep', 'tp'), pairs)  9.72 us
    pallas_call x2, Pallas kernels, send_rows(): pl.pallas_call(partial(send_kernel, chunk * SLOTS), out_shape=jax.ShapeDt...  5.49 us
    pallas_call x2, Pallas kernels, combine(): pl.pallas_call(partial(combine_kernel, chunk * SLOTS), out_shape=jax.Shap...  4.51 us
    pallas_call x2, Pallas kernels, pack_sum(): pl.pallas_call(pack_kernel, out_shape=jax.ShapeDtypeStruct((rows, LANES),...  4.41 us
  transfers between devices with their start and end apart: 12, of which 9 were waited for; matrix products, arithmetic and copies ran while one was open for 3% of the time, Pallas kernels for 16%

profile of v3, /device:TPU:1, one launch (start us, length us, event | category | flops | bytes accessed | tf_op | source)
XLA Modules:
  0.0 156.3 jit_solution(6121676552728981383)
XLA Ops:
  0.6 2.8 %send_rows.3 = bf16[512,768]{1,0:T(8,128)(2,1)} custom-call(s32[1]{0:T(128)} %bitcast.2.own_ref, bf16[512,2048]{1,0:T(8,128)(2,1)} %rows_hbm.3, f32[1,2048]{1,0:T(1,128)} %bitcast.45, s32[2,512]{1,0:T(2,128)} %bitcast.37), custom_call_target="tpu_custom_call" | custom-call | flops 2000000000 | bytes 2100000 | tf_op jit(solution)/shard_map/send_rows/pallas_call | solution.py:170
  3.4 13.0 %all-to-all-start.2 = ((bf16[64,8,768]{2,1,0:T(8,128)(2,1)}), bf16[64,8,768]{2,1,0:T(8,128)(2,1)S(1)}, u32[]{:S(2)}, u32[]{:S(2)}) async-start(bf16[64,8,768]{2,1,0:T(8,128)(2,1)} %bitcast.44), calls=%async_computation.2 | async-start | bytes 1572864 | tf_op jit(solution)/shard_map/all_to_all | solution.py:410
  16.4 2.8 %collective-permute-start.1 = (bf16[2048,256]{1,0:T(8,128)(2,1)}, bf16[2048,256]{1,0:T(8,128)(2,1)}, u32[]{:S(2)}, u32[]{:S(2)}) collective-permute-start(bf16[2048,256]{1,0:T(8,128)(2,1)} %bitcast.7.refs_1_), channel_id=1, source_target_pairs={{0,1},{1,0},{2,3},{3,2},{4,7},{5,6},{6,5},{7,4},{8,9},{9,8},{10,11... | collective-permute-start | bytes 3145736 | tf_op jit(solution)/shard_map/ppermute | solution.py:48
  19.4 2.6 %collective-permute-start.3 = (bf16[256,2048]{1,0:T(8,128)(2,1)}, bf16[256,2048]{1,0:T(8,128)(2,1)}, u32[]{:S(2)}, u32[]{:S(2)}) collective-permute-start(bf16[256,2048]{1,0:T(8,128)(2,1)} %bitcast.9.refs_5_), channel_id=1, source_target_pairs={{0,1},{1,0},{2,3},{3,2},{4,7},{5,6},{6,5},{7,4},{8,9},{9,8},{10,11... | collective-permute-start | bytes 3145736 | tf_op jit(solution)/shard_map/ppermute | solution.py:48
  21.9 2.7 %send_rows.2 = bf16[512,768]{1,0:T(8,128)(2,1)} custom-call(s32[1]{0:T(128)} %bitcast.2.own_ref, bf16[512,2048]{1,0:T(8,128)(2,1)} %rows_hbm.3, f32[1,2048]{1,0:T(1,128)} %bitcast.46, s32[2,512]{1,0:T(2,128)} %bitcast.38), custom_call_target="tpu_custom_call" | custom-call | flops 2000000000 | bytes 2100000 | tf_op jit(solution)/shard_map/send_rows/pallas_call | solution.py:170
  24.6 14.8 %all-to-all-done.2 = bf16[64,8,768]{2,1,0:T(8,128)(2,1)S(1)} async-done(((bf16[64,8,768]{2,1,0:T(8,128)(2,1)}), bf16[64,8,768]{2,1,0:T(8,128)(2,1)S(1)}, u32[]{:S(2)}, u32[]{:S(2)}) %all-to-all-start.2) | async-done | bytes 786464 | tf_op jit(solution)/shard_map/all_to_all | solution.py:410
  39.4 5.9 %all-to-all-start = ((bf16[64,8,768]{2,1,0:T(8,128)(2,1)}), bf16[64,8,768]{2,1,0:T(8,128)(2,1)S(1)}, u32[]{:S(2)}, u32[]{:S(2)}) async-start(bf16[64,8,768]{2,1,0:T(8,128)(2,1)} %bitcast.43), calls=%async_computation | async-start | bytes 1572864 | tf_op jit(solution)/shard_map/all_to_all | solution.py:410
  46.7 11.8 %collective-permute-done.3.refs_6_ = bf16[256,2048]{1,0:T(8,128)(2,1)} collective-permute-done((bf16[256,2048]{1,0:T(8,128)(2,1)}, bf16[256,2048]{1,0:T(8,128)(2,1)}, u32[]{:S(2)}, u32[]{:S(2)}) %collective-permute-start.3) | collective-permute-done | bytes 1048608 | tf_op jit(solution)/shard_map/ppermute | solution.py:48
  58.6 3.9 %collective-permute-done.6.refs_0_ = bf16[512,768]{1,0:T(8,128)(2,1)S(1)} collective-permute-done((bf16[512,768]{1,0:T(8,128)(2,1)S(1)}, bf16[512,768]{1,0:T(8,128)(2,1)S(1)}, u32[]{:S(2)}, u32[]{:S(2)}) %collective-permute-start.6) | collective-permute-done | bytes 786464 | tf_op jit(solution)/shard_map/ppermute | solution.py:48
  62.5 3.9 %half_ffn.7 = bf16[192,2048]{1,0:T(8,128)(2,1)S(1)} custom-call(bf16[512,768]{1,0:T(8,128)(2,1)S(1)} %collective-permute-done.6.refs_0_, bf16[2048,256]{1,0:T(8,128)(2,1)} %bitcast.7.refs_1_, bf16[2048,256]{1,0:T(8,128)(2,1)} %bitcast.8.refs_2_, bf16[2048,256]{1,0:T(8,128)(2,1)} %collective-permute-done.1.refs_3_, ...), custom_call_target="tpu_custom_call" | custom-call | flops 3500000000 | bytes 7864320 | tf_op jit(solution)/shard_map/half_ffn/pallas_call | solution.py:318
  69.6 3.9 %half_ffn.6.a_ref = bf16[192,2048]{1,0:T(8,128)(2,1)S(1)} custom-call(bf16[512,768]{1,0:T(8,128)(2,1)S(1)} %bitcast.35, bf16[2048,256]{1,0:T(8,128)(2,1)} %bitcast.7.refs_1_, bf16[2048,256]{1,0:T(8,128)(2,1)} %bitcast.8.refs_2_, bf16[2048,256]{1,0:T(8,128)(2,1)} %collective-permute-done.1.refs_3_, bf16[2048,256]{1,0:T(8,128)(2,1)} %collective-permute-done.2.refs_4_, ...), custom_call_target="tpu_custom_call" | custom-call | flops 3500000000 | bytes 7864320 | tf_op jit(solution)/shard_map/half_ffn/pallas_call | solution.py:318
  73.6 4.2 %collective-permute-done.7.b_ref = bf16[192,2048]{1,0:T(8,128)(2,1)} collective-permute-done((bf16[192,2048]{1,0:T(8,128)(2,1)S(1)}, bf16[192,2048]{1,0:T(8,128)(2,1)}, u32[]{:S(2)}, u32[]{:S(2)}) %collective-permute-start.7) | collective-permute-done | bytes 786464 | tf_op jit(solution)/shard_map/ppermute | solution.py:48
  77.8 2.7 %pack_sum.3 = bf16[512,768]{1,0:T(8,128)(2,1)} custom-call(bf16[192,2048]{1,0:T(8,128)(2,1)S(1)} %half_ffn.6.a_ref, bf16[192,2048]{1,0:T(8,128)(2,1)} %collective-permute-done.7.b_ref), custom_call_target="tpu_custom_call" | custom-call | flops 800000000 | bytes 2359296 | tf_op jit(solution)/shard_map/pack_sum/pallas_call | solution.py:269
  80.5 13.0 %all-to-all-start.3 = ((bf16[64,8,768]{2,1,0:T(8,128)(2,1)}), bf16[64,8,768]{2,1,0:T(8,128)(2,1)S(1)}, u32[]{:S(2)}, u32[]{:S(2)}) async-start(bf16[64,8,768]{2,1,0:T(8,128)(2,1)} %bitcast.15), calls=%async_computation.3 | async-start | bytes 1572864 | tf_op jit(solution)/shard_map/all_to_all | solution.py:410
  93.6 1.9 %collective-permute-start = (bf16[15,1024]{1,0:T(8,128)(2,1)S(1)}, bf16[15,1024]{1,0:T(8,128)(2,1)S(1)}, u32[]{:S(2)}, u32[]{:S(2)}) collective-permute-start(bf16[15,1024]{1,0:T(8,128)(2,1)S(1)} %slice.52), channel_id=1, source_target_pairs={{0,1},{1,2},{2,3},{3,4},{4,5},{5,6},{6,7},{7,8},{8,9},{9,10},{10,1... | collective-permute-start | bytes 92168 | tf_op jit(solution)/shard_map/ppermute | solution.py:38
  95.6 3.9 %half_ffn.5 = bf16[192,2048]{1,0:T(8,128)(2,1)S(1)} custom-call(bf16[512,768]{1,0:T(8,128)(2,1)S(1)} %collective-permute-done.4.refs_0_, bf16[2048,256]{1,0:T(8,128)(2,1)} %bitcast.7.refs_1_, bf16[2048,256]{1,0:T(8,128)(2,1)} %bitcast.8.refs_2_, bf16[2048,256]{1,0:T(8,128)(2,1)} %collective-permute-done.1.refs_3_, ...), custom_call_target="tpu_custom_call" | custom-call | flops 3500000000 | bytes 7864320 | tf_op jit(solution)/shard_map/half_ffn/pallas_call | solution.py:318
  100.6 3.9 %half_ffn.4.a_ref = bf16[192,2048]{1,0:T(8,128)(2,1)S(1)} custom-call(bf16[512,768]{1,0:T(8,128)(2,1)S(1)} %bitcast.32, bf16[2048,256]{1,0:T(8,128)(2,1)} %bitcast.7.refs_1_, bf16[2048,256]{1,0:T(8,128)(2,1)} %bitcast.8.refs_2_, bf16[2048,256]{1,0:T(8,128)(2,1)} %collective-permute-done.1.refs_3_, bf16[2048,256]{1,0:T(8,128)(2,1)} %collective-permute-done.2.refs_4_, ...), custom_call_target="tpu_custom_call" | custom-call | flops 3500000000 | bytes 7864320 | tf_op jit(solution)/shard_map/half_ffn/pallas_call | solution.py:318
  104.5 6.2 %collective-permute-done.5.b_ref = bf16[192,2048]{1,0:T(8,128)(2,1)S(1)} collective-permute-done((bf16[192,2048]{1,0:T(8,128)(2,1)S(1)}, bf16[192,2048]{1,0:T(8,128)(2,1)S(1)}, u32[]{:S(2)}, u32[]{:S(2)}) %collective-permute-start.5) | collective-permute-done | bytes 786464 | tf_op jit(solution)/shard_map/ppermute | solution.py:48
  112.4 4.2 %all-to-all-done.3 = bf16[64,8,768]{2,1,0:T(8,128)(2,1)S(1)} async-done(((bf16[64,8,768]{2,1,0:T(8,128)(2,1)}), bf16[64,8,768]{2,1,0:T(8,128)(2,1)S(1)}, u32[]{:S(2)}, u32[]{:S(2)}) %all-to-all-start.3) | async-done | bytes 786464 | tf_op jit(solution)/shard_map/all_to_all | solution.py:410
  116.6 13.8 %all-to-all-start.1 = ((bf16[64,8,768]{2,1,0:T(8,128)(2,1)}), bf16[64,8,768]{2,1,0:T(8,128)(2,1)S(1)}, u32[]{:S(2)}, u32[]{:S(2)}) async-start(bf16[64,8,768]{2,1,0:T(8,128)(2,1)} %bitcast.10), calls=%async_computation.1 | async-start | bytes 1572864 | tf_op jit(solution)/shard_map/all_to_all | solution.py:410
  130.4 1.9 %fusion.5 = f32[8,256,128]{1,2,0:T(8,128)S(1)} fusion(bf16[8,128,128]{2,1,0:T(8,128)(2,1)S(1)} %copy-done, f32[1024]{0:T(1024)S(1)} %select_select_fusion, f32[256]{0:T(256)S(1)} %convert_add_fusion, pred[1024]{0:T(1024)(128)(4,1)S(1)} %get-tuple-element.5, pred[1024]{0:T(1024)(128)(4,1)S(1)} %get-tuple-element.4, ...), kind=kOutput, calls=%fused_computation.23 | convolution fusion | flops 73138176 | bytes 18097152 | tf_op jit(solution)/shard_map/tgc,gcd->tgd/dot_general | solution.py:462
  132.6 2.3 %convolution_convert_fusion = bf16[256,2048]{1,0:T(8,128)(2,1)} fusion(bf16[256,1024]{0,1:T(8,128)(2,1)S(1)} %fusion.3, bf16[1024,2048]{1,0:T(8,128)(2,1)S(1)} %copy-done.5), kind=kOutput, calls=%fused_computation | convolution fusion | flops 1074266112 | bytes 5767168 | tf_op jit(solution)/shard_map/dot_general | solution.py:77
  136.6 16.7 %all-to-all-done.1 = bf16[64,8,768]{2,1,0:T(8,128)(2,1)S(1)} async-done(((bf16[64,8,768]{2,1,0:T(8,128)(2,1)}), bf16[64,8,768]{2,1,0:T(8,128)(2,1)S(1)}, u32[]{:S(2)}, u32[]{:S(2)}) %all-to-all-start.1) | async-done | bytes 786464 | tf_op jit(solution)/shard_map/all_to_all | solution.py:410
  153.4 2.7 %combine.3 = bf16[128,2048]{1,0:T(8,128)(2,1)} custom-call(s32[1]{0:T(128)} %bitcast.2.own_ref, bf16[512,768]{1,0:T(8,128)(2,1)S(1)} %bitcast.36, s32[2,512]{1,0:T(2,128)S(1)} %bitcast.40, f32[2,512]{1,0:T(2,128)S(1)} %bitcast.42, f32[128,2048]{1,0:T(8,128)S(1)} %combine.2.refs_0_), custom_call_target="tpu_custom_call" | custom-call | flops 1500000000 | bytes 2100000 | tf_op jit(solution)/shard_map/combine/pallas_call | solution.py:387
  (31 shorter events, 9.4 us)
Async XLA Ops:
  0.6 129.8 %copy-start = (bf16[8,128,128]{2,1,0:T(8,128)(2,1)S(1)}, bf16[8,128,128]{2,1,0:T(8,128)(2,1)}, u32[]{:S(2)}) copy-start(bf16[8,128,128]{2,1,0:T(8,128)(2,1)} %param.12) | copy-start | bytes 786436
  3.4 36.0 %all-to-all-start.2 = ((bf16[64,8,768]{2,1,0:T(8,128)(2,1)}), bf16[64,8,768]{2,1,0:T(8,128)(2,1)S(1)}, u32[]{:S(2)}, u32[]{:S(2)}) async-start(bf16[64,8,768]{2,1,0:T(8,128)(2,1)} %bitcast.44), calls=%async_computation.2 | async-start | bytes 1572864 | tf_op jit(solution)/shard_map/all_to_all | solution.py:410
  16.4 30.3 %collective-permute-start.1 = (bf16[2048,256]{1,0:T(8,128)(2,1)}, bf16[2048,256]{1,0:T(8,128)(2,1)}, u32[]{:S(2)}, u32[]{:S(2)}) collective-permute-start(bf16[2048,256]{1,0:T(8,128)(2,1)} %bitcast.7.refs_1_), channel_id=1, source_target_pairs={{0,1},{1,0},{2,3},{3,2},{4,7},{5,6},{6,5},{7,4},{8,9},{9,8},{10,11... | collective-permute-start | bytes 3145736 | tf_op jit(solution)/shard_map/ppermute | solution.py:48
  19.3 27.5 %collective-permute-start.2 = (bf16[2048,256]{1,0:T(8,128)(2,1)}, bf16[2048,256]{1,0:T(8,128)(2,1)}, u32[]{:S(2)}, u32[]{:S(2)}) collective-permute-start(bf16[2048,256]{1,0:T(8,128)(2,1)} %bitcast.8.refs_2_), channel_id=1, source_target_pairs={{0,1},{1,0},{2,3},{3,2},{4,7},{5,6},{6,5},{7,4},{8,9},{9,8},{10,11... | collective-permute-start | bytes 3145736 | tf_op jit(solution)/shard_map/ppermute | solution.py:48
  19.4 39.2 %collective-permute-start.3 = (bf16[256,2048]{1,0:T(8,128)(2,1)}, bf16[256,2048]{1,0:T(8,128)(2,1)}, u32[]{:S(2)}, u32[]{:S(2)}) collective-permute-start(bf16[256,2048]{1,0:T(8,128)(2,1)} %bitcast.9.refs_5_), channel_id=1, source_target_pairs={{0,1},{1,0},{2,3},{3,2},{4,7},{5,6},{6,5},{7,4},{8,9},{9,8},{10,11... | collective-permute-start | bytes 3145736 | tf_op jit(solution)/shard_map/ppermute | solution.py:48
  39.4 28.9 %all-to-all-start = ((bf16[64,8,768]{2,1,0:T(8,128)(2,1)}), bf16[64,8,768]{2,1,0:T(8,128)(2,1)S(1)}, u32[]{:S(2)}, u32[]{:S(2)}) async-start(bf16[64,8,768]{2,1,0:T(8,128)(2,1)} %bitcast.43), calls=%async_computation | async-start | bytes 1572864 | tf_op jit(solution)/shard_map/all_to_all | solution.py:410
  45.3 17.1 %collective-permute-start.6 = (bf16[512,768]{1,0:T(8,128)(2,1)S(1)}, bf16[512,768]{1,0:T(8,128)(2,1)S(1)}, u32[]{:S(2)}, u32[]{:S(2)}) collective-permute-start(bf16[512,768]{1,0:T(8,128)(2,1)S(1)} %bitcast.34), channel_id=1, source_target_pairs={{0,3},{1,2},{2,1},{3,0},{4,5},{5,4},{6,7},{7,6},{8,11},{9,10},{10,... | collective-permute-start | bytes 2359304 | tf_op jit(solution)/shard_map/ppermute | solution.py:48
  66.4 11.3 %collective-permute-start.7 = (bf16[192,2048]{1,0:T(8,128)(2,1)S(1)}, bf16[192,2048]{1,0:T(8,128)(2,1)}, u32[]{:S(2)}, u32[]{:S(2)}) collective-permute-start(bf16[192,2048]{1,0:T(8,128)(2,1)S(1)} %half_ffn.7), channel_id=1, source_target_pairs={{0,3},{1,2},{2,1},{3,0},{4,5},{5,4},{6,7},{7,6},{8,11},{9,10},{10,... | collective-permute-start | bytes 2359304 | tf_op jit(solution)/shard_map/ppermute | solution.py:48
  68.3 27.2 %collective-permute-start.4 = (bf16[512,768]{1,0:T(8,128)(2,1)S(1)}, bf16[512,768]{1,0:T(8,128)(2,1)S(1)}, u32[]{:S(2)}, u32[]{:S(2)}) collective-permute-start(bf16[512,768]{1,0:T(8,128)(2,1)S(1)} %bitcast.31), channel_id=1, source_target_pairs={{0,3},{1,2},{2,1},{3,0},{4,5},{5,4},{6,7},{7,6},{8,11},{9,10},{10,... | collective-permute-start | bytes 2359304 | tf_op jit(solution)/shard_map/ppermute | solution.py:48
  80.5 13.1 %copy-start.3 = (bf16[256,1024]{1,0:T(8,128)(2,1)S(1)}, bf16[256,1024]{1,0:T(8,128)(2,1)}, u32[]{:S(2)}) copy-start(bf16[256,1024]{1,0:T(8,128)(2,1)} %param.11) | copy-start | bytes 1572868
  80.5 36.1 %all-to-all-start.3 = ((bf16[64,8,768]{2,1,0:T(8,128)(2,1)}), bf16[64,8,768]{2,1,0:T(8,128)(2,1)S(1)}, u32[]{:S(2)}, u32[]{:S(2)}) async-start(bf16[64,8,768]{2,1,0:T(8,128)(2,1)} %bitcast.15), calls=%async_computation.3 | async-start | bytes 1572864 | tf_op jit(solution)/shard_map/all_to_all | solution.py:410
  93.6 6.8 %collective-permute-start = (bf16[15,1024]{1,0:T(8,128)(2,1)S(1)}, bf16[15,1024]{1,0:T(8,128)(2,1)S(1)}, u32[]{:S(2)}, u32[]{:S(2)}) collective-permute-start(bf16[15,1024]{1,0:T(8,128)(2,1)S(1)} %slice.52), channel_id=1, source_target_pairs={{0,1},{1,2},{2,3},{3,4},{4,5},{5,6},{6,7},{7,8},{8,9},{9,10},{10,1... | collective-permute-start | bytes 92168 | tf_op jit(solution)/shard_map/ppermute | solution.py:38
  99.5 11.2 %collective-permute-start.5 = (bf16[192,2048]{1,0:T(8,128)(2,1)S(1)}, bf16[192,2048]{1,0:T(8,128)(2,1)S(1)}, u32[]{:S(2)}, u32[]{:S(2)}) collective-permute-start(bf16[192,2048]{1,0:T(8,128)(2,1)S(1)} %half_ffn.5), channel_id=1, source_target_pairs={{0,3},{1,2},{2,1},{3,0},{4,5},{5,4},{6,7},{7,6},{8,11},{9,10},{10,... | collective-permute-start | bytes 2359304 | tf_op jit(solution)/shard_map/ppermute | solution.py:48
  116.6 36.8 %all-to-all-start.1 = ((bf16[64,8,768]{2,1,0:T(8,128)(2,1)}), bf16[64,8,768]{2,1,0:T(8,128)(2,1)S(1)}, u32[]{:S(2)}, u32[]{:S(2)}) async-start(bf16[64,8,768]{2,1,0:T(8,128)(2,1)} %bitcast.10), calls=%async_computation.1 | async-start | bytes 1572864 | tf_op jit(solution)/shard_map/all_to_all | solution.py:410
  130.4 2.0 %copy-start.4 = (f32[1024]{0:T(1024)S(1)}, f32[1024]{0:T(1024)}, u32[]{:S(2)}) copy-start(f32[1024]{0:T(1024)} %param.13) | copy-start | bytes 12292
  130.4 2.2 %copy-start.5 = (bf16[1024,2048]{1,0:T(8,128)(2,1)S(1)}, bf16[1024,2048]{1,0:T(8,128)(2,1)}, u32[]{:S(2)}) copy-start(bf16[1024,2048]{1,0:T(8,128)(2,1)} %param.14) | copy-start | bytes 12582916
  132.6 2.3 %copy-start.1 = (s32[512,2]{0,1:T(2,128)S(1)}, s32[512,2]{0,1:T(2,128)}, u32[]{:S(2)}) copy-start(s32[512,2]{0,1:T(2,128)} %param.17) | copy-start | bytes 12292
  132.6 2.3 %copy-start.2 = (f32[512,2]{0,1:T(2,128)S(1)}, f32[512,2]{0,1:T(2,128)}, u32[]{:S(2)}) copy-start(f32[512,2]{0,1:T(2,128)} %param.18) | copy-start | bytes 12292

commit v4 on v3

--- a/solution.py
+++ b/solution.py
@@ -285,18 +285,14 @@
         for n, (source, ref) in enumerate(zip(sources, held))
     ]
     rows.start()
-    for copy in copies[:2]:
+    for copy in copies:
         copy.start()
     x_ref, ga_ref, ua_ref, gb_ref, ub_ref, da_ref, db_ref = held
     rows.wait()
-    for copy in copies[2:4]:
-        copy.start()
     unpack(x_ref, dense_ref)
     x = dense_ref[...]
     copies[0].wait()
     copies[1].wait()
-    for copy in copies[4:]:
-        copy.start()
     hidden_a = (jax.nn.silu(dot(x, ga_ref[...])) * dot(x, ua_ref[...])).astype(BF16)
     copies[2].wait()
     copies[3].wait()
@@ -434,8 +430,7 @@
     before = passed_along(pool_in[rows_here - (WMAX - 1) :], ("ep", "tp"), 1)
 
     gate, up, down = w_gate[0], w_up[0], w_down[0]
-    gate_b = swapped(gate, 0)
-    up_b = swapped(up, 0)
+    gate_b, up_b = swapped(gate, 0), swapped(up, 0)
     down_b = swapped(down, 0)
     ffn = lambda x: half_ffn(x, gate, gate_b, up, up_b, down, down_b)
 

time: 157 us -> 156 us (level)
  Pallas kernels: 30.2 us -> 28.4 us
    pallas_call x4, Pallas kernels: 15.8 us -> 14 us  [half_ffn(): pl.pallas_call(ffn_kernel, out_shape=jax.ShapeDtypeStruct((dense, WIDTH),...]
  transfers between devices with their start and end apart: 12 -> 12, of which waited for: 9 -> 9; matrix products, arithmetic and copies ran while one was open for 3% -> 3% of each run, Pallas kernels for 16% -> 15%
where the time goes in v4:
time: 156 us; the launch traced here: 155 us
  waiting for transfers between devices  64.3 us (41%)
  starting transfers between devices  56.8 us (36%)
  Pallas kernels  28.4 us (18%)
  matrix products  4.18 us (3%)
    all_to_all x4, starting transfers between devices, exchanged(): lax.all_to_all(rows.reshape(experts, SUB, LANES), 'ep', split_axis=0, con...  45.1 us
    all_to_all x4, waiting for transfers between devices, exchanged(): lax.all_to_all(rows.reshape(experts, SUB, LANES), 'ep', split_axis=0, con...  37.1 us
    ppermute x7, waiting for transfers between devices, swapped(): return lax.ppermute(array, ('ep', 'tp'), pairs)  26.1 us
    pallas_call x4, Pallas kernels, half_ffn(): pl.pallas_call(ffn_kernel, out_shape=jax.ShapeDtypeStruct((dense, WIDTH),...  14 us
    ppermute x7, starting transfers between devices, swapped(): return lax.ppermute(array, ('ep', 'tp'), pairs)  9.74 us
    pallas_call x2, Pallas kernels, send_rows(): pl.pallas_call(partial(send_kernel, chunk * SLOTS), out_shape=jax.ShapeDt...  5.49 us
    pallas_call x2, Pallas kernels, combine(): pl.pallas_call(partial(combine_kernel, chunk * SLOTS), out_shape=jax.Shap...  4.51 us
    pallas_call x2, Pallas kernels, pack_sum(): pl.pallas_call(pack_kernel, out_shape=jax.ShapeDtypeStruct((rows, LANES),...  4.41 us
  transfers between devices with their start and end apart: 12, of which 9 were waited for; matrix products, arithmetic and copies ran while one was open for 3% of the time, Pallas kernels for 15%

profile of v4, /device:TPU:1, one launch (start us, length us, event | category | flops | bytes accessed | tf_op | source)
XLA Modules:
  0.0 155.3 jit_solution(14040777922439963342)
XLA Ops:
  0.6 2.8 %send_rows.3 = bf16[512,768]{1,0:T(8,128)(2,1)} custom-call(s32[1]{0:T(128)} %bitcast.2.own_ref, bf16[512,2048]{1,0:T(8,128)(2,1)} %rows_hbm.3, f32[1,2048]{1,0:T(1,128)} %bitcast.45, s32[2,512]{1,0:T(2,128)} %bitcast.37), custom_call_target="tpu_custom_call" | custom-call | flops 2000000000 | bytes 2100000 | tf_op jit(solution)/shard_map/send_rows/pallas_call | solution.py:170
  3.4 13.0 %all-to-all-start.2 = ((bf16[64,8,768]{2,1,0:T(8,128)(2,1)}), bf16[64,8,768]{2,1,0:T(8,128)(2,1)S(1)}, u32[]{:S(2)}, u32[]{:S(2)}) async-start(bf16[64,8,768]{2,1,0:T(8,128)(2,1)} %bitcast.44), calls=%async_computation.2 | async-start | bytes 1572864 | tf_op jit(solution)/shard_map/all_to_all | solution.py:406
  16.4 2.8 %collective-permute-start.1 = (bf16[2048,256]{1,0:T(8,128)(2,1)}, bf16[2048,256]{1,0:T(8,128)(2,1)}, u32[]{:S(2)}, u32[]{:S(2)}) collective-permute-start(bf16[2048,256]{1,0:T(8,128)(2,1)} %bitcast.7.refs_1_), channel_id=1, source_target_pairs={{0,1},{1,0},{2,3},{3,2},{4,7},{5,6},{6,5},{7,4},{8,9},{9,8},{10,11... | collective-permute-start | bytes 3145736 | tf_op jit(solution)/shard_map/ppermute | solution.py:48
  19.4 2.6 %collective-permute-start.3 = (bf16[256,2048]{1,0:T(8,128)(2,1)}, bf16[256,2048]{1,0:T(8,128)(2,1)}, u32[]{:S(2)}, u32[]{:S(2)}) collective-permute-start(bf16[256,2048]{1,0:T(8,128)(2,1)} %bitcast.9.refs_5_), channel_id=1, source_target_pairs={{0,1},{1,0},{2,3},{3,2},{4,7},{5,6},{6,5},{7,4},{8,9},{9,8},{10,11... | collective-permute-start | bytes 3145736 | tf_op jit(solution)/shard_map/ppermute | solution.py:48
  21.9 2.7 %send_rows.2 = bf16[512,768]{1,0:T(8,128)(2,1)} custom-call(s32[1]{0:T(128)} %bitcast.2.own_ref, bf16[512,2048]{1,0:T(8,128)(2,1)} %rows_hbm.3, f32[1,2048]{1,0:T(1,128)} %bitcast.46, s32[2,512]{1,0:T(2,128)} %bitcast.38), custom_call_target="tpu_custom_call" | custom-call | flops 2000000000 | bytes 2100000 | tf_op jit(solution)/shard_map/send_rows/pallas_call | solution.py:170
  24.6 14.8 %all-to-all-done.2 = bf16[64,8,768]{2,1,0:T(8,128)(2,1)S(1)} async-done(((bf16[64,8,768]{2,1,0:T(8,128)(2,1)}), bf16[64,8,768]{2,1,0:T(8,128)(2,1)S(1)}, u32[]{:S(2)}, u32[]{:S(2)}) %all-to-all-start.2) | async-done | bytes 786464 | tf_op jit(solution)/shard_map/all_to_all | solution.py:406
  39.4 5.9 %all-to-all-start = ((bf16[64,8,768]{2,1,0:T(8,128)(2,1)}), bf16[64,8,768]{2,1,0:T(8,128)(2,1)S(1)}, u32[]{:S(2)}, u32[]{:S(2)}) async-start(bf16[64,8,768]{2,1,0:T(8,128)(2,1)} %bitcast.43), calls=%async_computation | async-start | bytes 1572864 | tf_op jit(solution)/shard_map/all_to_all | solution.py:406
  46.7 11.8 %collective-permute-done.3.refs_6_ = bf16[256,2048]{1,0:T(8,128)(2,1)} collective-permute-done((bf16[256,2048]{1,0:T(8,128)(2,1)}, bf16[256,2048]{1,0:T(8,128)(2,1)}, u32[]{:S(2)}, u32[]{:S(2)}) %collective-permute-start.3) | collective-permute-done | bytes 1048608 | tf_op jit(solution)/shard_map/ppermute | solution.py:48
  58.6 3.9 %collective-permute-done.6.refs_0_ = bf16[512,768]{1,0:T(8,128)(2,1)S(1)} collective-permute-done((bf16[512,768]{1,0:T(8,128)(2,1)S(1)}, bf16[512,768]{1,0:T(8,128)(2,1)S(1)}, u32[]{:S(2)}, u32[]{:S(2)}) %collective-permute-start.6) | collective-permute-done | bytes 786464 | tf_op jit(solution)/shard_map/ppermute | solution.py:48
  62.5 3.5 %half_ffn.7 = bf16[192,2048]{1,0:T(8,128)(2,1)S(1)} custom-call(bf16[512,768]{1,0:T(8,128)(2,1)S(1)} %collective-permute-done.6.refs_0_, bf16[2048,256]{1,0:T(8,128)(2,1)} %bitcast.7.refs_1_, bf16[2048,256]{1,0:T(8,128)(2,1)} %bitcast.8.refs_2_, bf16[2048,256]{1,0:T(8,128)(2,1)} %collective-permute-done.1.refs_3_, ...), custom_call_target="tpu_custom_call" | custom-call | flops 3500000000 | bytes 7864320 | tf_op jit(solution)/shard_map/half_ffn/pallas_call | solution.py:314
  69.6 3.5 %half_ffn.6.a_ref = bf16[192,2048]{1,0:T(8,128)(2,1)S(1)} custom-call(bf16[512,768]{1,0:T(8,128)(2,1)S(1)} %bitcast.35, bf16[2048,256]{1,0:T(8,128)(2,1)} %bitcast.7.refs_1_, bf16[2048,256]{1,0:T(8,128)(2,1)} %bitcast.8.refs_2_, bf16[2048,256]{1,0:T(8,128)(2,1)} %collective-permute-done.1.refs_3_, bf16[2048,256]{1,0:T(8,128)(2,1)} %collective-permute-done.2.refs_4_, ...), custom_call_target="tpu_custom_call" | custom-call | flops 3500000000 | bytes 7864320 | tf_op jit(solution)/shard_map/half_ffn/pallas_call | solution.py:314
  73.2 4.2 %collective-permute-done.7.b_ref = bf16[192,2048]{1,0:T(8,128)(2,1)} collective-permute-done((bf16[192,2048]{1,0:T(8,128)(2,1)S(1)}, bf16[192,2048]{1,0:T(8,128)(2,1)}, u32[]{:S(2)}, u32[]{:S(2)}) %collective-permute-start.7) | collective-permute-done | bytes 786464 | tf_op jit(solution)/shard_map/ppermute | solution.py:48
  77.3 2.7 %pack_sum.3 = bf16[512,768]{1,0:T(8,128)(2,1)} custom-call(bf16[192,2048]{1,0:T(8,128)(2,1)S(1)} %half_ffn.6.a_ref, bf16[192,2048]{1,0:T(8,128)(2,1)} %collective-permute-done.7.b_ref), custom_call_target="tpu_custom_call" | custom-call | flops 800000000 | bytes 2359296 | tf_op jit(solution)/shard_map/pack_sum/pallas_call | solution.py:269
  80.1 12.9 %all-to-all-start.3 = ((bf16[64,8,768]{2,1,0:T(8,128)(2,1)}), bf16[64,8,768]{2,1,0:T(8,128)(2,1)S(1)}, u32[]{:S(2)}, u32[]{:S(2)}) async-start(bf16[64,8,768]{2,1,0:T(8,128)(2,1)} %bitcast.15), calls=%async_computation.3 | async-start | bytes 1572864 | tf_op jit(solution)/shard_map/all_to_all | solution.py:406
  93.0 1.9 %collective-permute-start = (bf16[15,1024]{1,0:T(8,128)(2,1)S(1)}, bf16[15,1024]{1,0:T(8,128)(2,1)S(1)}, u32[]{:S(2)}, u32[]{:S(2)}) collective-permute-start(bf16[15,1024]{1,0:T(8,128)(2,1)S(1)} %slice.52), channel_id=1, source_target_pairs={{0,1},{1,2},{2,3},{3,4},{4,5},{5,6},{6,7},{7,8},{8,9},{9,10},{10,1... | collective-permute-start | bytes 92168 | tf_op jit(solution)/shard_map/ppermute | solution.py:38
  95.0 3.5 %half_ffn.5 = bf16[192,2048]{1,0:T(8,128)(2,1)S(1)} custom-call(bf16[512,768]{1,0:T(8,128)(2,1)S(1)} %collective-permute-done.4.refs_0_, bf16[2048,256]{1,0:T(8,128)(2,1)} %bitcast.7.refs_1_, bf16[2048,256]{1,0:T(8,128)(2,1)} %bitcast.8.refs_2_, bf16[2048,256]{1,0:T(8,128)(2,1)} %collective-permute-done.1.refs_3_, ...), custom_call_target="tpu_custom_call" | custom-call | flops 3500000000 | bytes 7864320 | tf_op jit(solution)/shard_map/half_ffn/pallas_call | solution.py:314
  100.0 3.5 %half_ffn.4.a_ref = bf16[192,2048]{1,0:T(8,128)(2,1)S(1)} custom-call(bf16[512,768]{1,0:T(8,128)(2,1)S(1)} %bitcast.32, bf16[2048,256]{1,0:T(8,128)(2,1)} %bitcast.7.refs_1_, bf16[2048,256]{1,0:T(8,128)(2,1)} %bitcast.8.refs_2_, bf16[2048,256]{1,0:T(8,128)(2,1)} %collective-permute-done.1.refs_3_, bf16[2048,256]{1,0:T(8,128)(2,1)} %collective-permute-done.2.refs_4_, ...), custom_call_target="tpu_custom_call" | custom-call | flops 3500000000 | bytes 7864320 | tf_op jit(solution)/shard_map/half_ffn/pallas_call | solution.py:314
  103.5 6.2 %collective-permute-done.5.b_ref = bf16[192,2048]{1,0:T(8,128)(2,1)S(1)} collective-permute-done((bf16[192,2048]{1,0:T(8,128)(2,1)S(1)}, bf16[192,2048]{1,0:T(8,128)(2,1)S(1)}, u32[]{:S(2)}, u32[]{:S(2)}) %collective-permute-start.5) | collective-permute-done | bytes 786464 | tf_op jit(solution)/shard_map/ppermute | solution.py:48
  111.4 4.6 %all-to-all-done.3 = bf16[64,8,768]{2,1,0:T(8,128)(2,1)S(1)} async-done(((bf16[64,8,768]{2,1,0:T(8,128)(2,1)}), bf16[64,8,768]{2,1,0:T(8,128)(2,1)S(1)}, u32[]{:S(2)}, u32[]{:S(2)}) %all-to-all-start.3) | async-done | bytes 786464 | tf_op jit(solution)/shard_map/all_to_all | solution.py:406
  116.0 13.4 %all-to-all-start.1 = ((bf16[64,8,768]{2,1,0:T(8,128)(2,1)}), bf16[64,8,768]{2,1,0:T(8,128)(2,1)S(1)}, u32[]{:S(2)}, u32[]{:S(2)}) async-start(bf16[64,8,768]{2,1,0:T(8,128)(2,1)} %bitcast.10), calls=%async_computation.1 | async-start | bytes 1572864 | tf_op jit(solution)/shard_map/all_to_all | solution.py:406
  129.4 1.9 %fusion.5 = f32[8,256,128]{1,2,0:T(8,128)S(1)} fusion(bf16[8,128,128]{2,1,0:T(8,128)(2,1)S(1)} %copy-done, f32[1024]{0:T(1024)S(1)} %select_select_fusion, f32[256]{0:T(256)S(1)} %convert_add_fusion, pred[1024]{0:T(1024)(128)(4,1)S(1)} %get-tuple-element.5, pred[1024]{0:T(1024)(128)(4,1)S(1)} %get-tuple-element.4, ...), kind=kOutput, calls=%fused_computation.23 | convolution fusion | flops 73138176 | bytes 18097152 | tf_op jit(solution)/shard_map/tgc,gcd->tgd/dot_general | solution.py:457
  131.6 2.3 %convolution_convert_fusion = bf16[256,2048]{1,0:T(8,128)(2,1)} fusion(bf16[256,1024]{0,1:T(8,128)(2,1)S(1)} %fusion.3, bf16[1024,2048]{1,0:T(8,128)(2,1)S(1)} %copy-done.5), kind=kOutput, calls=%fused_computation | convolution fusion | flops 1074266112 | bytes 5767168 | tf_op jit(solution)/shard_map/dot_general | solution.py:77
  135.6 16.7 %all-to-all-done.1 = bf16[64,8,768]{2,1,0:T(8,128)(2,1)S(1)} async-done(((bf16[64,8,768]{2,1,0:T(8,128)(2,1)}), bf16[64,8,768]{2,1,0:T(8,128)(2,1)S(1)}, u32[]{:S(2)}, u32[]{:S(2)}) %all-to-all-start.1) | async-done | bytes 786464 | tf_op jit(solution)/shard_map/all_to_all | solution.py:406
  152.3 2.7 %combine.3 = bf16[128,2048]{1,0:T(8,128)(2,1)} custom-call(s32[1]{0:T(128)} %bitcast.2.own_ref, bf16[512,768]{1,0:T(8,128)(2,1)S(1)} %bitcast.36, s32[2,512]{1,0:T(2,128)S(1)} %bitcast.40, f32[2,512]{1,0:T(2,128)S(1)} %bitcast.42, f32[128,2048]{1,0:T(8,128)S(1)} %combine.2.refs_0_), custom_call_target="tpu_custom_call" | custom-call | flops 1500000000 | bytes 2100000 | tf_op jit(solution)/shard_map/combine/pallas_call | solution.py:383
  (31 shorter events, 10.3 us)
Async XLA Ops:
  0.6 128.7 %copy-start = (bf16[8,128,128]{2,1,0:T(8,128)(2,1)S(1)}, bf16[8,128,128]{2,1,0:T(8,128)(2,1)}, u32[]{:S(2)}) copy-start(bf16[8,128,128]{2,1,0:T(8,128)(2,1)} %param.12) | copy-start | bytes 786436
  3.4 36.0 %all-to-all-start.2 = ((bf16[64,8,768]{2,1,0:T(8,128)(2,1)}), bf16[64,8,768]{2,1,0:T(8,128)(2,1)S(1)}, u32[]{:S(2)}, u32[]{:S(2)}) async-start(bf16[64,8,768]{2,1,0:T(8,128)(2,1)} %bitcast.44), calls=%async_computation.2 | async-start | bytes 1572864 | tf_op jit(solution)/shard_map/all_to_all | solution.py:406
  16.4 30.3 %collective-permute-start.1 = (bf16[2048,256]{1,0:T(8,128)(2,1)}, bf16[2048,256]{1,0:T(8,128)(2,1)}, u32[]{:S(2)}, u32[]{:S(2)}) collective-permute-start(bf16[2048,256]{1,0:T(8,128)(2,1)} %bitcast.7.refs_1_), channel_id=1, source_target_pairs={{0,1},{1,0},{2,3},{3,2},{4,7},{5,6},{6,5},{7,4},{8,9},{9,8},{10,11... | collective-permute-start | bytes 3145736 | tf_op jit(solution)/shard_map/ppermute | solution.py:48
  19.3 27.5 %collective-permute-start.2 = (bf16[2048,256]{1,0:T(8,128)(2,1)}, bf16[2048,256]{1,0:T(8,128)(2,1)}, u32[]{:S(2)}, u32[]{:S(2)}) collective-permute-start(bf16[2048,256]{1,0:T(8,128)(2,1)} %bitcast.8.refs_2_), channel_id=1, source_target_pairs={{0,1},{1,0},{2,3},{3,2},{4,7},{5,6},{6,5},{7,4},{8,9},{9,8},{10,11... | collective-permute-start | bytes 3145736 | tf_op jit(solution)/shard_map/ppermute | solution.py:48
  19.4 39.2 %collective-permute-start.3 = (bf16[256,2048]{1,0:T(8,128)(2,1)}, bf16[256,2048]{1,0:T(8,128)(2,1)}, u32[]{:S(2)}, u32[]{:S(2)}) collective-permute-start(bf16[256,2048]{1,0:T(8,128)(2,1)} %bitcast.9.refs_5_), channel_id=1, source_target_pairs={{0,1},{1,0},{2,3},{3,2},{4,7},{5,6},{6,5},{7,4},{8,9},{9,8},{10,11... | collective-permute-start | bytes 3145736 | tf_op jit(solution)/shard_map/ppermute | solution.py:48
  39.4 28.9 %all-to-all-start = ((bf16[64,8,768]{2,1,0:T(8,128)(2,1)}), bf16[64,8,768]{2,1,0:T(8,128)(2,1)S(1)}, u32[]{:S(2)}, u32[]{:S(2)}) async-start(bf16[64,8,768]{2,1,0:T(8,128)(2,1)} %bitcast.43), calls=%async_computation | async-start | bytes 1572864 | tf_op jit(solution)/shard_map/all_to_all | solution.py:406
  45.3 17.1 %collective-permute-start.6 = (bf16[512,768]{1,0:T(8,128)(2,1)S(1)}, bf16[512,768]{1,0:T(8,128)(2,1)S(1)}, u32[]{:S(2)}, u32[]{:S(2)}) collective-permute-start(bf16[512,768]{1,0:T(8,128)(2,1)S(1)} %bitcast.34), channel_id=1, source_target_pairs={{0,3},{1,2},{2,1},{3,0},{4,5},{5,4},{6,7},{7,6},{8,11},{9,10},{10,... | collective-permute-start | bytes 2359304 | tf_op jit(solution)/shard_map/ppermute | solution.py:48
  66.0 11.3 %collective-permute-start.7 = (bf16[192,2048]{1,0:T(8,128)(2,1)S(1)}, bf16[192,2048]{1,0:T(8,128)(2,1)}, u32[]{:S(2)}, u32[]{:S(2)}) collective-permute-start(bf16[192,2048]{1,0:T(8,128)(2,1)S(1)} %half_ffn.7), channel_id=1, source_target_pairs={{0,3},{1,2},{2,1},{3,0},{4,5},{5,4},{6,7},{7,6},{8,11},{9,10},{10,... | collective-permute-start | bytes 2359304 | tf_op jit(solution)/shard_map/ppermute | solution.py:48
  68.3 26.6 %collective-permute-start.4 = (bf16[512,768]{1,0:T(8,128)(2,1)S(1)}, bf16[512,768]{1,0:T(8,128)(2,1)S(1)}, u32[]{:S(2)}, u32[]{:S(2)}) collective-permute-start(bf16[512,768]{1,0:T(8,128)(2,1)S(1)} %bitcast.31), channel_id=1, source_target_pairs={{0,3},{1,2},{2,1},{3,0},{4,5},{5,4},{6,7},{7,6},{8,11},{9,10},{10,... | collective-permute-start | bytes 2359304 | tf_op jit(solution)/shard_map/ppermute | solution.py:48
  80.1 12.9 %copy-start.3 = (bf16[256,1024]{1,0:T(8,128)(2,1)S(1)}, bf16[256,1024]{1,0:T(8,128)(2,1)}, u32[]{:S(2)}) copy-start(bf16[256,1024]{1,0:T(8,128)(2,1)} %param.11) | copy-start | bytes 1572868
  80.1 35.9 %all-to-all-start.3 = ((bf16[64,8,768]{2,1,0:T(8,128)(2,1)}), bf16[64,8,768]{2,1,0:T(8,128)(2,1)S(1)}, u32[]{:S(2)}, u32[]{:S(2)}) async-start(bf16[64,8,768]{2,1,0:T(8,128)(2,1)} %bitcast.15), calls=%async_computation.3 | async-start | bytes 1572864 | tf_op jit(solution)/shard_map/all_to_all | solution.py:406
  93.0 6.8 %collective-permute-start = (bf16[15,1024]{1,0:T(8,128)(2,1)S(1)}, bf16[15,1024]{1,0:T(8,128)(2,1)S(1)}, u32[]{:S(2)}, u32[]{:S(2)}) collective-permute-start(bf16[15,1024]{1,0:T(8,128)(2,1)S(1)} %slice.52), channel_id=1, source_target_pairs={{0,1},{1,2},{2,3},{3,4},{4,5},{5,6},{6,7},{7,8},{8,9},{9,10},{10,1... | collective-permute-start | bytes 92168 | tf_op jit(solution)/shard_map/ppermute | solution.py:38
  98.5 11.2 %collective-permute-start.5 = (bf16[192,2048]{1,0:T(8,128)(2,1)S(1)}, bf16[192,2048]{1,0:T(8,128)(2,1)S(1)}, u32[]{:S(2)}, u32[]{:S(2)}) collective-permute-start(bf16[192,2048]{1,0:T(8,128)(2,1)S(1)} %half_ffn.5), channel_id=1, source_target_pairs={{0,3},{1,2},{2,1},{3,0},{4,5},{5,4},{6,7},{7,6},{8,11},{9,10},{10,... | collective-permute-start | bytes 2359304 | tf_op jit(solution)/shard_map/ppermute | solution.py:48
  116.0 36.4 %all-to-all-start.1 = ((bf16[64,8,768]{2,1,0:T(8,128)(2,1)}), bf16[64,8,768]{2,1,0:T(8,128)(2,1)S(1)}, u32[]{:S(2)}, u32[]{:S(2)}) async-start(bf16[64,8,768]{2,1,0:T(8,128)(2,1)} %bitcast.10), calls=%async_computation.1 | async-start | bytes 1572864 | tf_op jit(solution)/shard_map/all_to_all | solution.py:406
  129.4 2.0 %copy-start.4 = (f32[1024]{0:T(1024)S(1)}, f32[1024]{0:T(1024)}, u32[]{:S(2)}) copy-start(f32[1024]{0:T(1024)} %param.13) | copy-start | bytes 12292
  129.4 2.2 %copy-start.5 = (bf16[1024,2048]{1,0:T(8,128)(2,1)S(1)}, bf16[1024,2048]{1,0:T(8,128)(2,1)}, u32[]{:S(2)}) copy-start(bf16[1024,2048]{1,0:T(8,128)(2,1)} %param.14) | copy-start | bytes 12582916
  131.6 2.3 %copy-start.1 = (s32[512,2]{0,1:T(2,128)S(1)}, s32[512,2]{0,1:T(2,128)}, u32[]{:S(2)}) copy-start(s32[512,2]{0,1:T(2,128)} %param.17) | copy-start | bytes 12292
  131.6 2.3 %copy-start.2 = (f32[512,2]{0,1:T(2,128)S(1)}, f32[512,2]{0,1:T(2,128)}, u32[]{:S(2)}) copy-start(f32[512,2]{0,1:T(2,128)} %param.18) | copy-start | bytes 12292

commit v5 on v4

--- a/solution.py
+++ b/solution.py
@@ -280,25 +280,41 @@
 
 def ffn_kernel(*refs):
     sources, out_ref, dense_ref, held, sems = refs[:7], refs[7], refs[8], refs[9:16], refs[16]
-    rows, *copies = [
-        pltpu.make_async_copy(source, ref, sems.at[n])
-        for n, (source, ref) in enumerate(zip(sources, held))
-    ]
-    rows.start()
+
+    def fetch(n, source, ref):
+        half = source.shape[0] // 2
+        return [
+            pltpu.make_async_copy(
+                source.at[pl.ds(part * half, half)], ref.at[pl.ds(part * half, half)], sems.at[2 * n + part]
+            )
+            for part in range(2)
+        ]
+
+    rows, *copies = [fetch(n, *pair) for n, pair in enumerate(zip(sources, held))]
+    for part in rows:
+        part.start()
     for copy in copies:
-        copy.start()
+        for part in copy:
+            part.start()
     x_ref, ga_ref, ua_ref, gb_ref, ub_ref, da_ref, db_ref = held
-    rows.wait()
+    for part in rows:
+        part.wait()
     unpack(x_ref, dense_ref)
     x = dense_ref[...]
-    copies[0].wait()
-    copies[1].wait()
+    for part in copies[0]:
+        part.wait()
+    for part in copies[1]:
+        part.wait()
     hidden_a = (jax.nn.silu(dot(x, ga_ref[...])) * dot(x, ua_ref[...])).astype(BF16)
-    copies[2].wait()
-    copies[3].wait()
+    for part in copies[2]:
+        part.wait()
+    for part in copies[3]:
+        part.wait()
     hidden_b = (jax.nn.silu(dot(x, gb_ref[...])) * dot(x, ub_ref[...])).astype(BF16)
-    copies[4].wait()
-    copies[5].wait()
+    for part in copies[4]:
+        part.wait()
+    for part in copies[5]:
+        part.wait()
     step = 2 * PIECE
     for c in range(WIDTH // step):
         columns = slice(c * step, (c + 1) * step)
@@ -318,7 +334,7 @@
         out_specs=VMEM,
         scratch_shapes=[pltpu.VMEM((dense, WIDTH), BF16)]
         + [pltpu.VMEM(operand.shape, BF16) for operand in operands]
-        + [pltpu.SemaphoreType.DMA((7,))],
+        + [pltpu.SemaphoreType.DMA((14,))],
         cost_estimate=pl.CostEstimate(
             flops=3_500_000_000,
             bytes_accessed=x.size * 4 + 6 * ga.size * 2,

time: 156 us -> 157 us (level)
  transfers between devices with their start and end apart: 12 -> 12, of which waited for: 9 -> 9; matrix products, arithmetic and copies ran while one was open for 3% -> 3% of each run, Pallas kernels for 15% -> 16%
where the time goes in v5:
time: 157 us; the launch traced here: 156 us
  waiting for transfers between devices  63.3 us (40%)
  starting transfers between devices  57.3 us (36%)
  Pallas kernels  29.8 us (19%)
  matrix products  4.18 us (3%)
    all_to_all x4, starting transfers between devices, exchanged(): lax.all_to_all(rows.reshape(experts, SUB, LANES), 'ep', split_axis=0, con...  45.7 us
    all_to_all x4, waiting for transfers between devices, exchanged(): lax.all_to_all(rows.reshape(experts, SUB, LANES), 'ep', split_axis=0, con...  36.4 us
    ppermute x7, waiting for transfers between devices, swapped(): return lax.ppermute(array, ('ep', 'tp'), pairs)  26.1 us
    pallas_call x4, Pallas kernels, half_ffn(): pl.pallas_call(ffn_kernel, out_shape=jax.ShapeDtypeStruct((dense, WIDTH),...  15.4 us
    ppermute x7, starting transfers between devices, swapped(): return lax.ppermute(array, ('ep', 'tp'), pairs)  9.74 us
    pallas_call x2, Pallas kernels, send_rows(): pl.pallas_call(partial(send_kernel, chunk * SLOTS), out_shape=jax.ShapeDt...  5.49 us
    pallas_call x2, Pallas kernels, combine(): pl.pallas_call(partial(combine_kernel, chunk * SLOTS), out_shape=jax.Shap...  4.51 us
    pallas_call x2, Pallas kernels, pack_sum(): pl.pallas_call(pack_kernel, out_shape=jax.ShapeDtypeStruct((rows, LANES),...  4.42 us
  transfers between devices with their start and end apart: 12, of which 9 were waited for; matrix products, arithmetic and copies ran while one was open for 3% of the time, Pallas kernels for 16%

profile of v5, /device:TPU:1, one launch (start us, length us, event | category | flops | bytes accessed | tf_op | source)
XLA Modules:
  0.0 156.1 jit_solution(10065327797734101610)
XLA Ops:
  0.6 2.8 %send_rows.3 = bf16[512,768]{1,0:T(8,128)(2,1)} custom-call(s32[1]{0:T(128)} %bitcast.2.own_ref, bf16[512,2048]{1,0:T(8,128)(2,1)} %rows_hbm.3, f32[1,2048]{1,0:T(1,128)} %bitcast.45, s32[2,512]{1,0:T(2,128)} %bitcast.37), custom_call_target="tpu_custom_call" | custom-call | flops 2000000000 | bytes 2100000 | tf_op jit(solution)/shard_map/send_rows/pallas_call | solution.py:170
  3.4 13.0 %all-to-all-start.2 = ((bf16[64,8,768]{2,1,0:T(8,128)(2,1)}), bf16[64,8,768]{2,1,0:T(8,128)(2,1)S(1)}, u32[]{:S(2)}, u32[]{:S(2)}) async-start(bf16[64,8,768]{2,1,0:T(8,128)(2,1)} %bitcast.44), calls=%async_computation.2 | async-start | bytes 1572864 | tf_op jit(solution)/shard_map/all_to_all | solution.py:422
  16.4 2.8 %collective-permute-start.1 = (bf16[2048,256]{1,0:T(8,128)(2,1)}, bf16[2048,256]{1,0:T(8,128)(2,1)}, u32[]{:S(2)}, u32[]{:S(2)}) collective-permute-start(bf16[2048,256]{1,0:T(8,128)(2,1)} %bitcast.7.refs_1_), channel_id=1, source_target_pairs={{0,1},{1,0},{2,3},{3,2},{4,7},{5,6},{6,5},{7,4},{8,9},{9,8},{10,11... | collective-permute-start | bytes 3145736 | tf_op jit(solution)/shard_map/ppermute | solution.py:48
  19.4 2.6 %collective-permute-start.3 = (bf16[256,2048]{1,0:T(8,128)(2,1)}, bf16[256,2048]{1,0:T(8,128)(2,1)}, u32[]{:S(2)}, u32[]{:S(2)}) collective-permute-start(bf16[256,2048]{1,0:T(8,128)(2,1)} %bitcast.9.refs_5_), channel_id=1, source_target_pairs={{0,1},{1,0},{2,3},{3,2},{4,7},{5,6},{6,5},{7,4},{8,9},{9,8},{10,11... | collective-permute-start | bytes 3145736 | tf_op jit(solution)/shard_map/ppermute | solution.py:48
  21.9 2.7 %send_rows.2 = bf16[512,768]{1,0:T(8,128)(2,1)} custom-call(s32[1]{0:T(128)} %bitcast.2.own_ref, bf16[512,2048]{1,0:T(8,128)(2,1)} %rows_hbm.3, f32[1,2048]{1,0:T(1,128)} %bitcast.46, s32[2,512]{1,0:T(2,128)} %bitcast.38), custom_call_target="tpu_custom_call" | custom-call | flops 2000000000 | bytes 2100000 | tf_op jit(solution)/shard_map/send_rows/pallas_call | solution.py:170
  24.6 14.8 %all-to-all-done.2 = bf16[64,8,768]{2,1,0:T(8,128)(2,1)S(1)} async-done(((bf16[64,8,768]{2,1,0:T(8,128)(2,1)}), bf16[64,8,768]{2,1,0:T(8,128)(2,1)S(1)}, u32[]{:S(2)}, u32[]{:S(2)}) %all-to-all-start.2) | async-done | bytes 786464 | tf_op jit(solution)/shard_map/all_to_all | solution.py:422
  39.4 5.9 %all-to-all-start = ((bf16[64,8,768]{2,1,0:T(8,128)(2,1)}), bf16[64,8,768]{2,1,0:T(8,128)(2,1)S(1)}, u32[]{:S(2)}, u32[]{:S(2)}) async-start(bf16[64,8,768]{2,1,0:T(8,128)(2,1)} %bitcast.43), calls=%async_computation | async-start | bytes 1572864 | tf_op jit(solution)/shard_map/all_to_all | solution.py:422
  46.7 11.8 %collective-permute-done.3.refs_6_ = bf16[256,2048]{1,0:T(8,128)(2,1)} collective-permute-done((bf16[256,2048]{1,0:T(8,128)(2,1)}, bf16[256,2048]{1,0:T(8,128)(2,1)}, u32[]{:S(2)}, u32[]{:S(2)}) %collective-permute-start.3) | collective-permute-done | bytes 1048608 | tf_op jit(solution)/shard_map/ppermute | solution.py:48
  58.6 3.9 %collective-permute-done.6.refs_0_ = bf16[512,768]{1,0:T(8,128)(2,1)S(1)} collective-permute-done((bf16[512,768]{1,0:T(8,128)(2,1)S(1)}, bf16[512,768]{1,0:T(8,128)(2,1)S(1)}, u32[]{:S(2)}, u32[]{:S(2)}) %collective-permute-start.6) | collective-permute-done | bytes 786464 | tf_op jit(solution)/shard_map/ppermute | solution.py:48
  62.5 3.8 %half_ffn.7 = bf16[192,2048]{1,0:T(8,128)(2,1)S(1)} custom-call(bf16[512,768]{1,0:T(8,128)(2,1)S(1)} %collective-permute-done.6.refs_0_, bf16[2048,256]{1,0:T(8,128)(2,1)} %bitcast.7.refs_1_, bf16[2048,256]{1,0:T(8,128)(2,1)} %bitcast.8.refs_2_, bf16[2048,256]{1,0:T(8,128)(2,1)} %collective-permute-done.1.refs_3_, ...), custom_call_target="tpu_custom_call" | custom-call | flops 3500000000 | bytes 7864320 | tf_op jit(solution)/shard_map/half_ffn/pallas_call | solution.py:330
  69.6 3.9 %half_ffn.6.a_ref = bf16[192,2048]{1,0:T(8,128)(2,1)S(1)} custom-call(bf16[512,768]{1,0:T(8,128)(2,1)S(1)} %bitcast.35, bf16[2048,256]{1,0:T(8,128)(2,1)} %bitcast.7.refs_1_, bf16[2048,256]{1,0:T(8,128)(2,1)} %bitcast.8.refs_2_, bf16[2048,256]{1,0:T(8,128)(2,1)} %collective-permute-done.1.refs_3_, bf16[2048,256]{1,0:T(8,128)(2,1)} %collective-permute-done.2.refs_4_, ...), custom_call_target="tpu_custom_call" | custom-call | flops 3500000000 | bytes 7864320 | tf_op jit(solution)/shard_map/half_ffn/pallas_call | solution.py:330
  73.5 4.2 %collective-permute-done.7.b_ref = bf16[192,2048]{1,0:T(8,128)(2,1)} collective-permute-done((bf16[192,2048]{1,0:T(8,128)(2,1)S(1)}, bf16[192,2048]{1,0:T(8,128)(2,1)}, u32[]{:S(2)}, u32[]{:S(2)}) %collective-permute-start.7) | collective-permute-done | bytes 786464 | tf_op jit(solution)/shard_map/ppermute | solution.py:48
  77.7 2.7 %pack_sum.3 = bf16[512,768]{1,0:T(8,128)(2,1)} custom-call(bf16[192,2048]{1,0:T(8,128)(2,1)S(1)} %half_ffn.6.a_ref, bf16[192,2048]{1,0:T(8,128)(2,1)} %collective-permute-done.7.b_ref), custom_call_target="tpu_custom_call" | custom-call | flops 800000000 | bytes 2359296 | tf_op jit(solution)/shard_map/pack_sum/pallas_call | solution.py:269
  80.4 13.1 %all-to-all-start.3 = ((bf16[64,8,768]{2,1,0:T(8,128)(2,1)}), bf16[64,8,768]{2,1,0:T(8,128)(2,1)S(1)}, u32[]{:S(2)}, u32[]{:S(2)}) async-start(bf16[64,8,768]{2,1,0:T(8,128)(2,1)} %bitcast.15), calls=%async_computation.3 | async-start | bytes 1572864 | tf_op jit(solution)/shard_map/all_to_all | solution.py:422
  93.5 1.9 %collective-permute-start = (bf16[15,1024]{1,0:T(8,128)(2,1)S(1)}, bf16[15,1024]{1,0:T(8,128)(2,1)S(1)}, u32[]{:S(2)}, u32[]{:S(2)}) collective-permute-start(bf16[15,1024]{1,0:T(8,128)(2,1)S(1)} %slice.52), channel_id=1, source_target_pairs={{0,1},{1,2},{2,3},{3,4},{4,5},{5,6},{6,7},{7,8},{8,9},{9,10},{10,1... | collective-permute-start | bytes 92168 | tf_op jit(solution)/shard_map/ppermute | solution.py:38
  95.5 3.9 %half_ffn.5 = bf16[192,2048]{1,0:T(8,128)(2,1)S(1)} custom-call(bf16[512,768]{1,0:T(8,128)(2,1)S(1)} %collective-permute-done.4.refs_0_, bf16[2048,256]{1,0:T(8,128)(2,1)} %bitcast.7.refs_1_, bf16[2048,256]{1,0:T(8,128)(2,1)} %bitcast.8.refs_2_, bf16[2048,256]{1,0:T(8,128)(2,1)} %collective-permute-done.1.refs_3_, ...), custom_call_target="tpu_custom_call" | custom-call | flops 3500000000 | bytes 7864320 | tf_op jit(solution)/shard_map/half_ffn/pallas_call | solution.py:330
  100.5 3.9 %half_ffn.4.a_ref = bf16[192,2048]{1,0:T(8,128)(2,1)S(1)} custom-call(bf16[512,768]{1,0:T(8,128)(2,1)S(1)} %bitcast.32, bf16[2048,256]{1,0:T(8,128)(2,1)} %bitcast.7.refs_1_, bf16[2048,256]{1,0:T(8,128)(2,1)} %bitcast.8.refs_2_, bf16[2048,256]{1,0:T(8,128)(2,1)} %collective-permute-done.1.refs_3_, bf16[2048,256]{1,0:T(8,128)(2,1)} %collective-permute-done.2.refs_4_, ...), custom_call_target="tpu_custom_call" | custom-call | flops 3500000000 | bytes 7864320 | tf_op jit(solution)/shard_map/half_ffn/pallas_call | solution.py:330
  104.4 6.2 %collective-permute-done.5.b_ref = bf16[192,2048]{1,0:T(8,128)(2,1)S(1)} collective-permute-done((bf16[192,2048]{1,0:T(8,128)(2,1)S(1)}, bf16[192,2048]{1,0:T(8,128)(2,1)S(1)}, u32[]{:S(2)}, u32[]{:S(2)}) %collective-permute-start.5) | collective-permute-done | bytes 786464 | tf_op jit(solution)/shard_map/ppermute | solution.py:48
  112.3 4.2 %all-to-all-done.3 = bf16[64,8,768]{2,1,0:T(8,128)(2,1)S(1)} async-done(((bf16[64,8,768]{2,1,0:T(8,128)(2,1)}), bf16[64,8,768]{2,1,0:T(8,128)(2,1)S(1)}, u32[]{:S(2)}, u32[]{:S(2)}) %all-to-all-start.3) | async-done | bytes 786464 | tf_op jit(solution)/shard_map/all_to_all | solution.py:422
  116.5 13.7 %all-to-all-start.1 = ((bf16[64,8,768]{2,1,0:T(8,128)(2,1)}), bf16[64,8,768]{2,1,0:T(8,128)(2,1)S(1)}, u32[]{:S(2)}, u32[]{:S(2)}) async-start(bf16[64,8,768]{2,1,0:T(8,128)(2,1)} %bitcast.10), calls=%async_computation.1 | async-start | bytes 1572864 | tf_op jit(solution)/shard_map/all_to_all | solution.py:422
  130.3 1.9 %fusion.5 = f32[8,256,128]{1,2,0:T(8,128)S(1)} fusion(bf16[8,128,128]{2,1,0:T(8,128)(2,1)S(1)} %copy-done, f32[1024]{0:T(1024)S(1)} %select_select_fusion, f32[256]{0:T(256)S(1)} %convert_add_fusion, pred[1024]{0:T(1024)(128)(4,1)S(1)} %get-tuple-element.5, pred[1024]{0:T(1024)(128)(4,1)S(1)} %get-tuple-element.4, ...), kind=kOutput, calls=%fused_computation.23 | convolution fusion | flops 73138176 | bytes 18097152 | tf_op jit(solution)/shard_map/tgc,gcd->tgd/dot_general | solution.py:473
  132.4 2.3 %convolution_convert_fusion = bf16[256,2048]{1,0:T(8,128)(2,1)} fusion(bf16[256,1024]{0,1:T(8,128)(2,1)S(1)} %fusion.3, bf16[1024,2048]{1,0:T(8,128)(2,1)S(1)} %copy-done.5), kind=kOutput, calls=%fused_computation | convolution fusion | flops 1074266112 | bytes 5767168 | tf_op jit(solution)/shard_map/dot_general | solution.py:77
  136.5 16.7 %all-to-all-done.1 = bf16[64,8,768]{2,1,0:T(8,128)(2,1)S(1)} async-done(((bf16[64,8,768]{2,1,0:T(8,128)(2,1)}), bf16[64,8,768]{2,1,0:T(8,128)(2,1)S(1)}, u32[]{:S(2)}, u32[]{:S(2)}) %all-to-all-start.1) | async-done | bytes 786464 | tf_op jit(solution)/shard_map/all_to_all | solution.py:422
  153.2 2.7 %combine.3 = bf16[128,2048]{1,0:T(8,128)(2,1)} custom-call(s32[1]{0:T(128)} %bitcast.2.own_ref, bf16[512,768]{1,0:T(8,128)(2,1)S(1)} %bitcast.36, s32[2,512]{1,0:T(2,128)S(1)} %bitcast.40, f32[2,512]{1,0:T(2,128)S(1)} %bitcast.42, f32[128,2048]{1,0:T(8,128)S(1)} %combine.2.refs_0_), custom_call_target="tpu_custom_call" | custom-call | flops 1500000000 | bytes 2100000 | tf_op jit(solution)/shard_map/combine/pallas_call | solution.py:399
  (31 shorter events, 9.6 us)
Async XLA Ops:
  0.6 129.6 %copy-start = (bf16[8,128,128]{2,1,0:T(8,128)(2,1)S(1)}, bf16[8,128,128]{2,1,0:T(8,128)(2,1)}, u32[]{:S(2)}) copy-start(bf16[8,128,128]{2,1,0:T(8,128)(2,1)} %param.12) | copy-start | bytes 786436
  3.4 36.0 %all-to-all-start.2 = ((bf16[64,8,768]{2,1,0:T(8,128)(2,1)}), bf16[64,8,768]{2,1,0:T(8,128)(2,1)S(1)}, u32[]{:S(2)}, u32[]{:S(2)}) async-start(bf16[64,8,768]{2,1,0:T(8,128)(2,1)} %bitcast.44), calls=%async_computation.2 | async-start | bytes 1572864 | tf_op jit(solution)/shard_map/all_to_all | solution.py:422
  16.4 30.3 %collective-permute-start.1 = (bf16[2048,256]{1,0:T(8,128)(2,1)}, bf16[2048,256]{1,0:T(8,128)(2,1)}, u32[]{:S(2)}, u32[]{:S(2)}) collective-permute-start(bf16[2048,256]{1,0:T(8,128)(2,1)} %bitcast.7.refs_1_), channel_id=1, source_target_pairs={{0,1},{1,0},{2,3},{3,2},{4,7},{5,6},{6,5},{7,4},{8,9},{9,8},{10,11... | collective-permute-start | bytes 3145736 | tf_op jit(solution)/shard_map/ppermute | solution.py:48
  19.3 27.5 %collective-permute-start.2 = (bf16[2048,256]{1,0:T(8,128)(2,1)}, bf16[2048,256]{1,0:T(8,128)(2,1)}, u32[]{:S(2)}, u32[]{:S(2)}) collective-permute-start(bf16[2048,256]{1,0:T(8,128)(2,1)} %bitcast.8.refs_2_), channel_id=1, source_target_pairs={{0,1},{1,0},{2,3},{3,2},{4,7},{5,6},{6,5},{7,4},{8,9},{9,8},{10,11... | collective-permute-start | bytes 3145736 | tf_op jit(solution)/shard_map/ppermute | solution.py:48
  19.4 39.2 %collective-permute-start.3 = (bf16[256,2048]{1,0:T(8,128)(2,1)}, bf16[256,2048]{1,0:T(8,128)(2,1)}, u32[]{:S(2)}, u32[]{:S(2)}) collective-permute-start(bf16[256,2048]{1,0:T(8,128)(2,1)} %bitcast.9.refs_5_), channel_id=1, source_target_pairs={{0,1},{1,0},{2,3},{3,2},{4,7},{5,6},{6,5},{7,4},{8,9},{9,8},{10,11... | collective-permute-start | bytes 3145736 | tf_op jit(solution)/shard_map/ppermute | solution.py:48
  39.4 28.9 %all-to-all-start = ((bf16[64,8,768]{2,1,0:T(8,128)(2,1)}), bf16[64,8,768]{2,1,0:T(8,128)(2,1)S(1)}, u32[]{:S(2)}, u32[]{:S(2)}) async-start(bf16[64,8,768]{2,1,0:T(8,128)(2,1)} %bitcast.43), calls=%async_computation | async-start | bytes 1572864 | tf_op jit(solution)/shard_map/all_to_all | solution.py:422
  45.3 17.1 %collective-permute-start.6 = (bf16[512,768]{1,0:T(8,128)(2,1)S(1)}, bf16[512,768]{1,0:T(8,128)(2,1)S(1)}, u32[]{:S(2)}, u32[]{:S(2)}) collective-permute-start(bf16[512,768]{1,0:T(8,128)(2,1)S(1)} %bitcast.34), channel_id=1, source_target_pairs={{0,3},{1,2},{2,1},{3,0},{4,5},{5,4},{6,7},{7,6},{8,11},{9,10},{10,... | collective-permute-start | bytes 2359304 | tf_op jit(solution)/shard_map/ppermute | solution.py:48
  66.3 11.3 %collective-permute-start.7 = (bf16[192,2048]{1,0:T(8,128)(2,1)S(1)}, bf16[192,2048]{1,0:T(8,128)(2,1)}, u32[]{:S(2)}, u32[]{:S(2)}) collective-permute-start(bf16[192,2048]{1,0:T(8,128)(2,1)S(1)} %half_ffn.7), channel_id=1, source_target_pairs={{0,3},{1,2},{2,1},{3,0},{4,5},{5,4},{6,7},{7,6},{8,11},{9,10},{10,... | collective-permute-start | bytes 2359304 | tf_op jit(solution)/shard_map/ppermute | solution.py:48
  68.3 27.1 %collective-permute-start.4 = (bf16[512,768]{1,0:T(8,128)(2,1)S(1)}, bf16[512,768]{1,0:T(8,128)(2,1)S(1)}, u32[]{:S(2)}, u32[]{:S(2)}) collective-permute-start(bf16[512,768]{1,0:T(8,128)(2,1)S(1)} %bitcast.31), channel_id=1, source_target_pairs={{0,3},{1,2},{2,1},{3,0},{4,5},{5,4},{6,7},{7,6},{8,11},{9,10},{10,... | collective-permute-start | bytes 2359304 | tf_op jit(solution)/shard_map/ppermute | solution.py:48
  80.4 13.1 %copy-start.3 = (bf16[256,1024]{1,0:T(8,128)(2,1)S(1)}, bf16[256,1024]{1,0:T(8,128)(2,1)}, u32[]{:S(2)}) copy-start(bf16[256,1024]{1,0:T(8,128)(2,1)} %param.11) | copy-start | bytes 1572868
  80.4 36.1 %all-to-all-start.3 = ((bf16[64,8,768]{2,1,0:T(8,128)(2,1)}), bf16[64,8,768]{2,1,0:T(8,128)(2,1)S(1)}, u32[]{:S(2)}, u32[]{:S(2)}) async-start(bf16[64,8,768]{2,1,0:T(8,128)(2,1)} %bitcast.15), calls=%async_computation.3 | async-start | bytes 1572864 | tf_op jit(solution)/shard_map/all_to_all | solution.py:422
  93.5 6.8 %collective-permute-start = (bf16[15,1024]{1,0:T(8,128)(2,1)S(1)}, bf16[15,1024]{1,0:T(8,128)(2,1)S(1)}, u32[]{:S(2)}, u32[]{:S(2)}) collective-permute-start(bf16[15,1024]{1,0:T(8,128)(2,1)S(1)} %slice.52), channel_id=1, source_target_pairs={{0,1},{1,2},{2,3},{3,4},{4,5},{5,6},{6,7},{7,8},{8,9},{9,10},{10,1... | collective-permute-start | bytes 92168 | tf_op jit(solution)/shard_map/ppermute | solution.py:38
  99.4 11.2 %collective-permute-start.5 = (bf16[192,2048]{1,0:T(8,128)(2,1)S(1)}, bf16[192,2048]{1,0:T(8,128)(2,1)S(1)}, u32[]{:S(2)}, u32[]{:S(2)}) collective-permute-start(bf16[192,2048]{1,0:T(8,128)(2,1)S(1)} %half_ffn.5), channel_id=1, source_target_pairs={{0,3},{1,2},{2,1},{3,0},{4,5},{5,4},{6,7},{7,6},{8,11},{9,10},{10,... | collective-permute-start | bytes 2359304 | tf_op jit(solution)/shard_map/ppermute | solution.py:48
  116.5 36.7 %all-to-all-start.1 = ((bf16[64,8,768]{2,1,0:T(8,128)(2,1)}), bf16[64,8,768]{2,1,0:T(8,128)(2,1)S(1)}, u32[]{:S(2)}, u32[]{:S(2)}) async-start(bf16[64,8,768]{2,1,0:T(8,128)(2,1)} %bitcast.10), calls=%async_computation.1 | async-start | bytes 1572864 | tf_op jit(solution)/shard_map/all_to_all | solution.py:422
  130.2 2.0 %copy-start.4 = (f32[1024]{0:T(1024)S(1)}, f32[1024]{0:T(1024)}, u32[]{:S(2)}) copy-start(f32[1024]{0:T(1024)} %param.13) | copy-start | bytes 12292
  130.2 2.2 %copy-start.5 = (bf16[1024,2048]{1,0:T(8,128)(2,1)S(1)}, bf16[1024,2048]{1,0:T(8,128)(2,1)}, u32[]{:S(2)}) copy-start(bf16[1024,2048]{1,0:T(8,128)(2,1)} %param.14) | copy-start | bytes 12582916
  132.4 2.3 %copy-start.1 = (s32[512,2]{0,1:T(2,128)S(1)}, s32[512,2]{0,1:T(2,128)}, u32[]{:S(2)}) copy-start(s32[512,2]{0,1:T(2,128)} %param.17) | copy-start | bytes 12292
  132.4 2.3 %copy-start.2 = (f32[512,2]{0,1:T(2,128)S(1)}, f32[512,2]{0,1:T(2,128)}, u32[]{:S(2)}) copy-start(f32[512,2]{0,1:T(2,128)} %param.18) | copy-start | bytes 12292
